TPU v7x, 256 devices: a whole 4x4x8 slice. The times are simulated.
256 devices in a mesh: fs: 32 (over z, x), tp: 8 (over y, core).
Axes of the slice: x: 4, y: 4, z: 8, core: 2. Of those that a mesh axis runs over, the one named last changes fastest.
Arguments:
- tokens: bfloat16 [16384, 2048], P('fs', 'tp'), may hold values from -16 to 16
- pre_mix_gain: bfloat16 [2048], P('tp'), may hold values from 0.099609375 to 1.8984375
- w_gate_in: bfloat16 [2048, 2048], P('fs', 'tp'), may hold values from -0.125 to 0.125
- w_input: bfloat16 [2048, 2048], P('fs', 'tp'), may hold values from -0.125 to 0.125
- mix_kernel: bfloat16 [4, 2048], P(None, 'tp'), may hold values from -3 to 3
- w_recur: bfloat16 [8, 256, 256], P('tp'), may hold values from -0.375 to 0.375
- w_inject: bfloat16 [8, 256, 256], P('tp'), may hold values from -0.375 to 0.375
- decay_param: float32 [2048], P('tp'), may hold values from 3 to 13
- w_mix_out: bfloat16 [2048, 2048], P('tp', 'fs'), may hold values from -0.125 to 0.125
- post_mix_gain: bfloat16 [2048], P('tp'), may hold values from 0.099609375 to 1.8984375
- pre_ffn_gain: bfloat16 [2048], P('tp'), may hold values from 0.099609375 to 1.8984375
- w_up_gate: bfloat16 [2048, 5632], P('fs', 'tp'), may hold values from -0.125 to 0.125
- w_up_value: bfloat16 [2048, 5632], P('fs', 'tp'), may hold values from -0.125 to 0.125
- gate_kernel: bfloat16 [3, 5632], P(None, 'tp'), may hold values from -3 to 3
- value_kernel: bfloat16 [3, 5632], P(None, 'tp'), may hold values from -3 to 3
- w_down: bfloat16 [5632, 2048], P('tp', 'fs'), may hold values from -0.078125 to 0.078125
- post_ffn_gain: bfloat16 [2048], P('tp'), may hold values from 0.099609375 to 1.8984375
Outputs:
- layer_out: bfloat16 [16384, 2048], P('fs', 'tp')
All inputs are finite; a program needn't handle non-finite values.
Results may differ from a plain program's by a relative error of at most 0.015.
Values may be sent and summed in bfloat16 or wider, within the bound.
No kernel may reach another device: no remote copies, remote signals or barrier semaphores. Data moves between devices by JAX's collectives and lax.ppermute only.
A program may use at most 64 MiB of HBM per device.

v0:
```python
import jax
import jax.numpy as jnp
from jax import lax
from jax.experimental import pallas as pl
from jax.experimental.pallas import tpu as pltpu
from jax.sharding import Mesh
from jax.sharding import PartitionSpec as P


D = 2048
FS = ("z", "x")
TP = ("y", "c")
NZ, NX, NY, NC = 8, 4, 4, 2
NTP = NY * NC
ROWS = 512
OWN = ROWS // NTP
PIECE = D // NTP
EXTRA = 16
UNITS = 704
norm_eps = 1e-06
gate_power = 8.0
bf16, f32 = jnp.bfloat16, jnp.float32


def moved(value, axis, n, by):
    return lax.ppermute(value, axis, [(i, (i + by) % n) for i in range(n)])


def ring_gathered(block, axis, n):
    got = [block] + [None] * (n - 1)
    ahead = back = block
    for s in range(1, n // 2):
        ahead = moved(ahead, axis, n, 1)
        back = moved(back, axis, n, -1)
        got[s], got[n - s] = ahead, back
    far = jnp.where(lax.axis_index("c") == 0, ahead, back)
    got[n // 2] = spread(far, axis, n)
    return got


def in_order(blocks, axis, dim):
    n, me = len(blocks), lax.axis_index(axis)
    shape = blocks[0].shape
    whole = jnp.zeros((*shape[:dim], n, *shape[dim:]), blocks[0].dtype)
    for k in [1, 0, *range(2, n)]:
        start = [0] * whole.ndim
        start[dim] = lax.rem(me + (n - k), n)
        whole = lax.dynamic_update_slice(whole, jnp.expand_dims(blocks[k], dim), start)
    return whole


def swapped(value):
    return lax.ppermute(value, "c", [(0, 1), (1, 0)])


def spread(value, axis, n):
    pairs = [(2 * i, 2 * ((i + 1) % n)) for i in range(n)]
    pairs += [(2 * i + 1, 2 * ((i - 1) % n) + 1) for i in range(n)]
    return lax.ppermute(value, (axis, "c"), pairs)


def ring_pieces(pack, axis, n):
    p = [pack]
    for _ in range(1, n // 2):
        p.append(spread(p[-1], axis, n))
    return p, spread(p[-1][0], axis, n)


def rows_ring(pack):
    p, far = ring_pieces(pack, "y", NY)
    return [p[0], p[1], far, swapped(p[1]), swapped(far)]


Y_ORDER = (
    (0, 0, 0, 0), (0, 1, 0, 1), (1, 0, 1, 0), (1, 1, 1, 1),
    (2, None, 2, 0), (4, None, 2, 1), (3, 1, 3, 0), (3, 0, 3, 1),
)


def reduced_rows(give, keep_far, keep_next, home):
    given = swapped(give).astype(f32)
    far = (keep_far.astype(f32) + given[:OWN]).astype(bf16)
    far = spread(far, "y", NY)
    follow = keep_next.astype(f32) + given[OWN:]
    follow = jnp.concatenate([follow[:OWN] + far.astype(f32), follow[OWN:]], axis=0).astype(bf16)
    return (home.astype(f32) + spread(follow, "y", NY).astype(f32)).astype(bf16)


def gelu(v):
    return 0.5 * v * (1.0 + jnp.tanh(0.7978845608028654 * (v + 0.044715 * v * v * v)))


def one_less_exp(u):
    s = 1.0 + u * (1.0 / 8.0)
    for k in range(7, 1, -1):
        s = 1.0 + u * (1.0 / k) * s
    return jnp.where(u > -0.5, -u * s, 1.0 - jnp.exp(u))


def stretch(index, size):
    return pl.ds(pl.multiple_of(index * size, size), size)


def upstream(axis, n, k):
    sign = 1 - 2 * lax.axis_index("c")
    return lax.rem(lax.axis_index(axis) + n - k * sign, n)


def core(rel):
    return lax.axis_index("c") if rel == 0 else 1 - lax.axis_index("c")


def dot_nt(a, b):
    return lax.dot_general(a, b, (((1,), (1,)), ((), ())), preferred_element_type=f32)


def projected(hid_ref, turned_ref, wout_ref, outs):
    my = lax.axis_index("y")
    sign = 1 - 2 * lax.axis_index("c")
    ahead, behind = lax.rem(my + NY + sign, NY), lax.rem(my + NY - sign, NY)
    across = lax.rem(my + 2, NY)
    order = [
        (across, 1), (behind, 1), (behind, 0), (across, 0), (ahead, 0), (ahead, 1), (my, 0), (my, 1),
    ]
    for i, (chip, rel) in enumerate(order):
        turned_ref[i * OWN : (i + 1) * OWN, :] = hid_ref[stretch(chip * NC + core(rel), OWN), :]

    def columns(k, _):
        at = stretch(k, PIECE)
        part = dot_nt(turned_ref[...], wout_ref[at, :]).astype(bf16)
        first = 0
        for ref in outs:
            ref[:, at] = part[first : first + ref.shape[0], :]
            first += ref.shape[0]
        return 0

    lax.fori_loop(0, NTP, columns, 0)


def behind(me, by, n):
    return lax.rem(me + (n - by), n)


def mixer_kernel(*refs):
    x_refs, w_refs = refs[0:5], refs[5:9]
    taps_ref, recur_ref, inject_ref, slope_ref = refs[9:13]
    outs, own_ref, gain_ref = refs[13:17], refs[17], refs[18]
    v_ref, win_ref, wout_ref, gate_ref, in_ref, keep_ref, drive_ref, hid_ref, turned_ref = refs[19:]
    mz, mx = lax.axis_index("z"), lax.axis_index("x")

    def placed(kz, _):
        for kx in range(NX):
            z, x = lax.rem(mz + NZ - kz, NZ), behind(mx, kx, NX)
            at = pl.ds(pl.multiple_of((z * NX + x) * 64, 64), 64)
            win_ref[at, :] = w_refs[kx][kz, :, 0:512]
            wout_ref[at, :] = w_refs[kx][kz, :, 512:]
        return 0

    lax.fori_loop(0, NZ, placed, 0)
    xs = []
    for operand, entry, ky, rel in Y_ORDER:
        ref = x_refs[operand] if entry is None else x_refs[operand].at[entry]
        xs.append((ref, stretch(upstream("y", NY, ky) * NC + core(rel), PIECE)))
    for ref, at in xs:
        for rel in (0, 1):
            own_ref[rel * OWN : (rel + 1) * OWN, at] = ref[
                stretch(lax.axis_index("y") * NC + core(rel), OWN), :
            ]
        gain_ref[:, at] = ref[ROWS : ROWS + 8, :]

    def normed(i, _):
        rows = stretch(i, 64)
        squares = jnp.zeros((64, 1), f32)
        for ref, _at in xs:
            v = ref[rows, :].astype(f32)
            squares = squares + jnp.sum(v * v, axis=1, keepdims=True)
        factor = lax.rsqrt(squares / D + norm_eps)
        for ref, at in xs:
            gain = ref[ROWS : ROWS + 1, :].astype(f32)
            v_ref[rows, at] = (ref[rows, :].astype(f32) * factor * gain).astype(bf16)
        return 0

    lax.fori_loop(0, ROWS // 64, normed, 0)
    gate_ref[...] = jnp.dot(
        v_ref[...], win_ref[:, 0:PIECE], preferred_element_type=f32
    ).astype(bf16)
    in_ref[0:TOP, :] = jnp.zeros((TOP, PIECE), bf16)
    in_ref[TOP:, :] = jnp.dot(
        v_ref[...], win_ref[:, PIECE:], preferred_element_type=f32
    ).astype(bf16)
    taps = taps_ref[...].astype(f32)
    within = lax.broadcasted_iota(jnp.int32, (CHUNK, PIECE), 0) % 8

    def chunk(i, carry):
        first = pl.multiple_of(i * CHUNK, CHUNK)
        rows = pl.ds(first, CHUNK)
        v = in_ref[pl.ds(first, CHUNK + TOP), :].astype(f32)
        smoothed = v[TOP:] * taps[3:4, :]
        for back in (1, 2, 3):
            smoothed = smoothed + pltpu.roll(v, back, 0)[TOP:] * taps[3 - back : 4 - back, :]
        smoothed = smoothed.astype(bf16)
        recur = jax.nn.sigmoid(jnp.dot(smoothed, recur_ref[...], preferred_element_type=f32))
        inject = jax.nn.sigmoid(jnp.dot(smoothed, inject_ref[...], preferred_element_type=f32))
        log_retain = -gate_power * recur * slope_ref[...]
        keep = jnp.exp(log_retain)
        drive = jnp.sqrt(one_less_exp(2.0 * log_retain)) * inject * smoothed.astype(f32)
        for by in (1, 2, 4):
            ok = within >= by
            drive = jnp.where(ok, keep * pltpu.roll(drive, by, 0), 0.0) + drive
            keep = jnp.where(ok, pltpu.roll(keep, by, 0), 1.0) * keep
        keep_ref[...] = keep
        drive_ref[...] = drive
        for t in range(CHUNK // 8):
            at = slice(8 * t, 8 * t + 8)
            state = keep_ref[at, :] * carry + drive_ref[at, :]
            drive_ref[at, :] = state
            carry = state[7:8, :]
        hid_ref[rows, :] = (gelu(gate_ref[rows, :].astype(f32)) * drive_ref[...]).astype(bf16)
        return carry

    lax.fori_loop(0, ROWS // CHUNK, chunk, jnp.zeros((1, PIECE), f32))
    projected(hid_ref, turned_ref, wout_ref, outs)


CHUNK = 128
TOP = 16
VMEM = pl.BlockSpec(memory_space=pltpu.VMEM)
PARTS = tuple(jax.ShapeDtypeStruct((n * OWN, D), bf16) for n in (3, 1, 2, 2))
PAIR = jax.ShapeDtypeStruct((2 * OWN, D), bf16)


def mixer(operands):
    return pl.pallas_call(
        mixer_kernel,
        out_shape=(*PARTS, PAIR, jax.ShapeDtypeStruct((8, D), bf16)),
        in_specs=[VMEM] * len(operands),
        out_specs=(VMEM,) * 6,
        scratch_shapes=[
            pltpu.VMEM((ROWS, D), bf16),
            pltpu.VMEM((D, 512), bf16),
            pltpu.VMEM((D, PIECE), bf16),
            pltpu.VMEM((ROWS, PIECE), bf16),
            pltpu.VMEM((ROWS + TOP, PIECE), bf16),
            pltpu.VMEM((CHUNK, PIECE), f32),
            pltpu.VMEM((CHUNK, PIECE), f32),
            pltpu.VMEM((ROWS, PIECE), bf16),
            pltpu.VMEM((ROWS, PIECE), bf16),
        ],
        compiler_params=pltpu.CompilerParams(vmem_limit_bytes=24 * 1024 * 1024),
        cost_estimate=pl.CostEstimate(
            flops=2 * ROWS * D * 768 + 4 * ROWS * PIECE * PIECE,
            bytes_accessed=8 * 1024 * 1024, transcendentals=ROWS * PIECE * 6,
        ),
        name="mixer",
    )(*operands)


def row_normed(widened, row_gain):
    factor = lax.rsqrt(jnp.sum(widened * widened, axis=1, keepdims=True) / D + norm_eps)
    return widened * factor * row_gain.astype(f32)


UP_CUT = 256
UP_CUTS = 6


def ffn_kernel(*refs):
    n_refs, up_w, down_w, taps_ref = refs[0:5], refs[5], refs[6], refs[7]
    outs = refs[8:12]
    n_all, up_ref, act_ref, turned_ref = refs[12:]
    for operand, entry, ky, rel in Y_ORDER:
        ref = n_refs[operand] if entry is None else n_refs[operand].at[entry]
        n_all[stretch(upstream("y", NY, ky) * NC + core(rel), OWN), :] = ref[...]
    up_ref[0:TOP, :] = jnp.zeros((TOP, 2 * UNITS), bf16)

    def up(at):
        up_ref[TOP:, at] = jnp.dot(
            n_all[...], up_w[:, at], preferred_element_type=f32
        ).astype(bf16)

    def loop(i, _):
        up(stretch(i, UP_CUT))
        return 0

    lax.fori_loop(0, UP_CUTS - 1, loop, 0)
    up(pl.ds((UP_CUTS - 1) * UP_CUT, 128))
    taps = taps_ref[...].astype(f32)

    def smooth(i, _):
        at = pl.multiple_of(i * 64, 64)
        v = up_ref[pl.ds(at, 64 + TOP), :].astype(f32)
        conv = v[TOP:] * taps[2:3, :]
        for back in (1, 2):
            conv = conv + pltpu.roll(v, back, 0)[TOP:] * taps[2 - back : 3 - back, :]
        act_ref[pl.ds(at, 64), :] = (gelu(conv[:, 0:UNITS]) * conv[:, UNITS:]).astype(bf16)
        return 0

    lax.fori_loop(0, ROWS // 64, smooth, 0)
    projected(act_ref, turned_ref, down_w, outs)


def ffn(operands):
    return pl.pallas_call(
        ffn_kernel,
        out_shape=PARTS,
        in_specs=[VMEM] * 8,
        out_specs=(VMEM,) * 4,
        scratch_shapes=[
            pltpu.VMEM((ROWS, D), bf16),
            pltpu.VMEM((ROWS + TOP, 2 * UNITS), bf16),
            pltpu.VMEM((ROWS, UNITS), bf16),
            pltpu.VMEM((ROWS, UNITS), bf16),
        ],
        compiler_params=pltpu.CompilerParams(vmem_limit_bytes=28 * 1024 * 1024),
        cost_estimate=pl.CostEstimate(
            flops=2 * ROWS * D * 3 * UNITS, bytes_accessed=13 * 1024 * 1024,
            transcendentals=ROWS * UNITS,
        ),
        name="ffn",
    )(*operands)


def shards(
    tokens, pre_mix_gain, w_gate_in, w_input, mix_kernel, w_recur, w_inject, decay_param,
    w_mix_out, post_mix_gain, pre_ffn_gain, w_up_gate, w_up_value, gate_kernel, value_kernel,
    w_down, post_ffn_gain,
):
    z_own = jnp.concatenate([w_gate_in, w_input, w_mix_out.T, w_down.T], axis=1)
    along_z = ring_gathered(z_own, "z", NZ)
    gains = jnp.concatenate([pre_mix_gain, post_mix_gain, pre_ffn_gain, post_ffn_gain])
    gains = gains.reshape(4, PIECE)
    packed = jnp.concatenate([tokens, jnp.pad(gains, ((0, EXTRA - 4), (0, 0)))], axis=0)
    mix_blocks = ring_gathered(jnp.stack([b[:, :768] for b in along_z]), "x", NX)
    packed = jnp.stack([packed, swapped(packed)])
    x_blocks = rows_ring(packed)
    up_own = jnp.concatenate([w_up_gate, w_up_value], axis=1)
    sent = jnp.broadcast_to(up_own[None], (NX, *up_own.shape))
    along_x = lax.all_to_all(sent, "x", 0, 0, tiled=True)
    up_all = in_order(ring_gathered(along_x, "z", NZ), "z", 0).reshape(D, 2 * UNITS)
    down_z = in_order([b[:, 768:] for b in along_z], "z", 0)
    down_all = in_order(ring_gathered(down_z, "x", NX), "x", 1).reshape(D, UNITS)
    x_blocks[1], decay_param = lax.optimization_barrier((x_blocks[1], decay_param))
    slope = jax.nn.softplus(-decay_param)[None, :]
    *parts, own_rows, gain_rows = mixer(
        (*x_blocks, *mix_blocks, mix_kernel, w_recur[0], w_inject[0], slope)
    )
    part = reduced_rows(*parts)
    part, taps_of = lax.optimization_barrier((part, (gate_kernel, value_kernel)))
    taps = jnp.concatenate(taps_of, axis=1)
    turned = swapped(jnp.concatenate([part[OWN:], part[:OWN]], axis=0))
    mixer_sum = part.astype(f32) + turned.astype(f32)
    middle = (own_rows.astype(f32) + row_normed(mixer_sum, gain_rows[1:2])).astype(bf16)
    normed = row_normed(middle.astype(f32), gain_rows[2:3]).astype(bf16).reshape(2, OWN, D)
    parts = ffn((*rows_ring(normed), up_all, down_all, taps))
    part = reduced_rows(*parts)
    ffn_sum = part[:OWN].astype(f32) + swapped(part[OWN:]).astype(f32)
    out_rows = middle[:OWN].astype(f32) + row_normed(ffn_sum, gain_rows[3:4])
    to_columns = out_rows.astype(bf16).reshape(OWN, NTP, PIECE).transpose(1, 0, 2)
    return lax.all_to_all(to_columns, TP, 0, 0, tiled=True).reshape(ROWS, PIECE)


def solution(mesh):
    finer = Mesh(mesh.devices.reshape(NZ, NX, NY, NC), ("z", "x", "y", "c"))
    return jax.shard_map(
        shards,
        mesh=finer,
        in_specs=(
            P(FS, TP), P(TP), P(FS, TP), P(FS, TP), P(None, TP), P(TP, None, None),
            P(TP, None, None), P(TP), P(TP, FS), P(TP), P(TP), P(FS, TP), P(FS, TP),
            P(None, TP), P(None, TP), P(TP, FS), P(TP),
        ),
        out_specs=P(FS, TP),
        check_vma=False,
    )
```

profile of v0, /device:TPU:1, one launch (start us, length us, event | category | flops | bytes accessed | tf_op | source)
XLA Modules:
  0.0 200.2 jit_solution(10503451208528047099)
XLA Ops:
  0.9 2.5 %collective-permute-start.5 = (bf16[64,1472]{1,0:T(8,128)(2,1)S(1)}, bf16[64,1472]{1,0:T(8,128)(2,1)}, u32[]{:S(2)}, u32[]{:S(2)}) collective-permute-start(bf16[64,1472]{1,0:T(8,128)(2,1)S(1)} %pad_maximum_fusion.4), channel_id=1, source_target_pairs={{0,32},{32,64},{64,96},{96,128},{128,160},{160,192},{192,224},{224... | collective-permute-start | bytes 565256 | tf_op jit(solution)/shard_map/ppermute | solution.py:26
  3.5 4.0 %collective-permute-start.8 = (bf16[64,1472]{1,0:T(8,128)(2,1)S(1)}, bf16[64,1472]{1,0:T(8,128)(2,1)}, u32[]{:S(2)}, u32[]{:S(2)}) collective-permute-start(bf16[64,1472]{1,0:T(8,128)(2,1)S(1)} %pad_maximum_fusion.4), channel_id=1, source_target_pairs={{0,224},{32,0},{64,32},{96,64},{128,96},{160,128},{192,160},{224,1... | collective-permute-start | bytes 565256 | tf_op jit(solution)/shard_map/ppermute | solution.py:26
  12.2 4.0 %all-to-all-start = ((bf16[4,64,1408]{2,1,0:T(8,128)(2,1)}), bf16[4,64,1408]{2,1,0:T(8,128)(2,1)S(1)}, u32[]{:S(2)}, u32[]{:S(2)}) async-start(bf16[4,64,1408]{2,1,0:T(8,128)(2,1)} %broadcast_in_dim.83), calls=%async_computation | async-start | bytes 1441792 | tf_op jit(solution)/shard_map/all_to_all | solution.py:338
  19.0 2.7 %collective-permute-start.9 = (bf16[64,1472]{1,0:T(8,128)(2,1)}, bf16[64,1472]{1,0:T(8,128)(2,1)}, u32[]{:S(2)}, u32[]{:S(2)}) collective-permute-start(bf16[64,1472]{1,0:T(8,128)(2,1)} %collective-permute-done.8), channel_id=1, source_target_pairs={{0,224},{32,0},{64,32},{96,64},{128,96},{160,128},{192,160},{224,1... | collective-permute-start | bytes 565256 | tf_op jit(solution)/shard_map/ppermute | solution.py:26
  24.2 2.8 %collective-permute-start.1 = (bf16[2,528,256]{2,1,0:T(8,128)(2,1)S(1)}, bf16[2,528,256]{2,1,0:T(8,128)(2,1)S(1)}, u32[]{:S(2)}, u32[]{:S(2)}) collective-permute-start(bf16[2,528,256]{2,1,0:T(8,128)(2,1)S(1)} %pad_maximum_fusion.refs_0_), channel_id=1, source_target_pairs={{0,2},{2,4},{4,6},{6,0},{1,7},{3,1},{5,3},{7,5},{8,10},{10,12},{12... | collective-permute-start | bytes 1622024 | tf_op jit(solution)/shard_map/ppermute | solution.py:59
  27.1 2.7 %collective-permute-start.10 = (bf16[64,1472]{1,0:T(8,128)(2,1)}, bf16[64,1472]{1,0:T(8,128)(2,1)}, u32[]{:S(2)}, u32[]{:S(2)}) collective-permute-start(bf16[64,1472]{1,0:T(8,128)(2,1)} %collective-permute-done.9), channel_id=1, source_target_pairs={{0,224},{32,0},{64,32},{96,64},{128,96},{160,128},{192,160},{224,1... | collective-permute-start | bytes 565256 | tf_op jit(solution)/shard_map/ppermute | solution.py:26
  31.6 2.7 %collective-permute-start.26 = (bf16[4,64,1408]{2,1,0:T(8,128)(2,1)S(1)}, bf16[4,64,1408]{2,1,0:T(8,128)(2,1)S(1)}, u32[]{:S(2)}, u32[]{:S(2)}) collective-permute-start(bf16[4,64,1408]{2,1,0:T(8,128)(2,1)S(1)} %all-to-all-done), channel_id=1, source_target_pairs={{0,224},{32,0},{64,32},{96,64},{128,96},{160,128},{192,160},{224,1... | collective-permute-start | bytes 2162696 | tf_op jit(solution)/shard_map/ppermute | solution.py:26
  35.3 2.5 %collective-permute-start.11 = (bf16[64,1472]{1,0:T(8,128)(2,1)S(1)}, bf16[64,1472]{1,0:T(8,128)(2,1)S(1)}, u32[]{:S(2)}, u32[]{:S(2)}) collective-permute-start(bf16[64,1472]{1,0:T(8,128)(2,1)S(1)} %broadcast_select_fusion.3), channel_id=1, source_target_pairs={{0,32},{32,64},{64,96},{96,128},{128,160},{160,192},{192,224},{224... | collective-permute-start | bytes 565256 | tf_op jit(solution)/shard_map/ppermute | solution.py:59
  39.5 12.9 %collective-permute-done.11 = bf16[64,1472]{1,0:T(8,128)(2,1)S(1)} collective-permute-done((bf16[64,1472]{1,0:T(8,128)(2,1)S(1)}, bf16[64,1472]{1,0:T(8,128)(2,1)S(1)}, u32[]{:S(2)}, u32[]{:S(2)}) %collective-permute-start.11) | collective-permute-done | bytes 188448 | tf_op jit(solution)/shard_map/ppermute | solution.py:59
  60.9 2.8 %collective-permute-start.31 = (bf16[8,64,704]{2,1,0:T(8,128)(2,1)S(1)}, bf16[8,64,704]{2,1,0:T(8,128)(2,1)S(1)}, u32[]{:S(2)}, u32[]{:S(2)}) collective-permute-start(bf16[8,64,704]{2,1,0:T(8,128)(2,1)S(1)} %fusion.9), channel_id=1, source_target_pairs={{0,24},{8,0},{16,8},{24,16},{1,25},{9,1},{17,9},{25,17},{2,26},{10... | collective-permute-start | bytes 2162696 | tf_op jit(solution)/shard_map/ppermute | solution.py:26
  64.5 9.8 %collective-permute-done.12.refs_6_ = bf16[8,64,768]{2,1,0:T(8,128)(2,1)S(1)} collective-permute-done((bf16[8,64,768]{2,1,0:T(8,128)(2,1)S(1)}, bf16[8,64,768]{2,1,0:T(8,128)(2,1)S(1)}, u32[]{:S(2)}, u32[]{:S(2)}) %collective-permute-start.12) | collective-permute-done | bytes 786464 | tf_op jit(solution)/shard_map/ppermute | solution.py:26
  77.2 2.8 %collective-permute-done.2.refs_2_ = bf16[528,256]{1,0:T(8,128)(2,1)S(1)} collective-permute-done((bf16[528,256]{1,0:T(8,128)(2,1)S(1)}, bf16[528,256]{1,0:T(8,128)(2,1)S(1)}, u32[]{:S(2)}, u32[]{:S(2)}) %collective-permute-start.2) | collective-permute-done | bytes 270368 | tf_op jit(solution)/shard_map/ppermute | solution.py:59
  80.0 5.5 %collective-permute-start.3 = (bf16[2,528,256]{2,1,0:T(8,128)(2,1)S(1)}, bf16[2,528,256]{2,1,0:T(8,128)(2,1)S(1)}, u32[]{:S(2)}, u32[]{:S(2)}) collective-permute-start(bf16[2,528,256]{2,1,0:T(8,128)(2,1)S(1)} %collective-permute-done.1.refs_1_), channel_id=1, source_target_pairs={{0,1},{1,0},{2,3},{3,2},{4,5},{5,4},{6,7},{7,6},{8,9},{9,8},{10,11... | collective-permute-start | bytes 1622024 | tf_op jit(solution)/shard_map/ppermute | solution.py:53
  85.5 5.7 %collective-permute-done.30 = bf16[8,64,704]{2,1,0:T(8,128)(2,1)S(1)} collective-permute-done((bf16[8,64,704]{2,1,0:T(8,128)(2,1)S(1)}, bf16[8,64,704]{2,1,0:T(8,128)(2,1)S(1)}, u32[]{:S(2)}, u32[]{:S(2)}) %collective-permute-start.30) | collective-permute-done | bytes 720928 | tf_op jit(solution)/shard_map/ppermute | solution.py:26
  92.7 3.4 %collective-permute-start.27 = (bf16[4,64,1408]{2,1,0:T(8,128)(2,1)S(1)}, bf16[4,64,1408]{2,1,0:T(8,128)(2,1)S(1)}, u32[]{:S(2)}, u32[]{:S(2)}) collective-permute-start(bf16[4,64,1408]{2,1,0:T(8,128)(2,1)S(1)} %collective-permute-done.26), channel_id=1, source_target_pairs={{0,224},{32,0},{64,32},{96,64},{128,96},{160,128},{192,160},{224,1... | collective-permute-start | bytes 2162696 | tf_op jit(solution)/shard_map/ppermute | solution.py:26
  98.1 3.3 %collective-permute-done.14.refs_7_ = bf16[8,64,768]{2,1,0:T(8,128)(2,1)S(1)} collective-permute-done((bf16[8,64,768]{2,1,0:T(8,128)(2,1)S(1)}, bf16[8,64,768]{2,1,0:T(8,128)(2,1)S(1)}, u32[]{:S(2)}, u32[]{:S(2)}) %collective-permute-start.14) | collective-permute-done | bytes 786464 | tf_op jit(solution)/shard_map/ppermute | solution.py:59
  101.5 7.9 %mixer.1 = (bf16[192,2048]{1,0:T(8,128)(2,1)S(1)}, bf16[64,2048]{1,0:T(8,128)(2,1)S(1)}, bf16[128,2048]{1,0:T(8,128)(2,1)S(1)}, bf16[128,2048]{1,0:T(8,128)(2,1)...) custom-call(bf16[2,528,256]{2,1,0:T(8,128)(2,1)S(1)} %pad_maximum_fusion.refs_0_, ...), custom_call_target="tpu_custom_call" | custom-call | flops 1744830464 | bytes 8388608 | tf_op jit(solution)/shard_map/mixer/pallas_call | solution.py:233
  109.7 2.7 %collective-permute-done.24 = bf16[4,64,1408]{2,1,0:T(8,128)(2,1)S(1)} collective-permute-done((bf16[4,64,1408]{2,1,0:T(8,128)(2,1)S(1)}, bf16[4,64,1408]{2,1,0:T(8,128)(2,1)S(1)}, u32[]{:S(2)}, u32[]{:S(2)}) %collective-permute-start.24) | collective-permute-done | bytes 720928 | tf_op jit(solution)/shard_map/ppermute | solution.py:26
  112.5 2.7 %collective-permute-start.28 = (bf16[4,64,1408]{2,1,0:T(8,128)(2,1)S(1)}, bf16[4,64,1408]{2,1,0:T(8,128)(2,1)S(1)}, u32[]{:S(2)}, u32[]{:S(2)}) collective-permute-start(bf16[4,64,1408]{2,1,0:T(8,128)(2,1)S(1)} %collective-permute-done.27), channel_id=1, source_target_pairs={{0,224},{32,0},{64,32},{96,64},{128,96},{160,128},{192,160},{224,1... | collective-permute-start | bytes 2162696 | tf_op jit(solution)/shard_map/ppermute | solution.py:26
  115.5 2.3 %collective-permute-start.16 = (bf16[64,2048]{1,0:T(8,128)(2,1)S(1)}, bf16[64,2048]{1,0:T(8,128)(2,1)S(1)}, u32[]{:S(2)}, u32[]{:S(2)}) collective-permute-start(bf16[64,2048]{1,0:T(8,128)(2,1)S(1)} %fusion.6), channel_id=1, source_target_pairs={{0,2},{2,4},{4,6},{6,0},{1,7},{3,1},{5,3},{7,5},{8,10},{10,12},{12... | collective-permute-start | bytes 786440 | tf_op jit(solution)/shard_map/ppermute | solution.py:59
  118.0 3.1 %collective-permute-done.16 = bf16[64,2048]{1,0:T(8,128)(2,1)S(1)} collective-permute-done((bf16[64,2048]{1,0:T(8,128)(2,1)S(1)}, bf16[64,2048]{1,0:T(8,128)(2,1)S(1)}, u32[]{:S(2)}, u32[]{:S(2)}) %collective-permute-start.16) | collective-permute-done | bytes 262176 | tf_op jit(solution)/shard_map/ppermute | solution.py:59
  121.2 3.5 %collective-permute-start.17 = (bf16[128,2048]{1,0:T(8,128)(2,1)S(1)}, bf16[128,2048]{1,0:T(8,128)(2,1)S(1)}, u32[]{:S(2)}, u32[]{:S(2)}) collective-permute-start(bf16[128,2048]{1,0:T(8,128)(2,1)S(1)} %pad_maximum_fusion.1), channel_id=1, source_target_pairs={{0,2},{2,4},{4,6},{6,0},{1,7},{3,1},{5,3},{7,5},{8,10},{10,12},{12... | collective-permute-start | bytes 1572872 | tf_op jit(solution)/shard_map/ppermute | solution.py:59
  124.8 6.0 %collective-permute-done.17 = bf16[128,2048]{1,0:T(8,128)(2,1)S(1)} collective-permute-done((bf16[128,2048]{1,0:T(8,128)(2,1)S(1)}, bf16[128,2048]{1,0:T(8,128)(2,1)S(1)}, u32[]{:S(2)}, u32[]{:S(2)}) %collective-permute-start.17) | collective-permute-done | bytes 524320 | tf_op jit(solution)/shard_map/ppermute | solution.py:59
  131.1 4.5 %collective-permute-start.18 = (bf16[128,2048]{1,0:T(8,128)(2,1)S(1)}, bf16[128,2048]{1,0:T(8,128)(2,1)S(1)}, u32[]{:S(2)}, u32[]{:S(2)}) collective-permute-start(bf16[128,2048]{1,0:T(8,128)(2,1)S(1)} %pad_maximum_fusion.2), channel_id=1, source_target_pairs={{0,1},{1,0},{2,3},{3,2},{4,5},{5,4},{6,7},{7,6},{8,9},{9,8},{10,11... | collective-permute-start | bytes 1572872 | tf_op jit(solution)/shard_map/ppermute | solution.py:53
  138.1 8.1 %collective-permute-done.29 = bf16[4,64,1408]{2,1,0:T(8,128)(2,1)S(1)} collective-permute-done((bf16[4,64,1408]{2,1,0:T(8,128)(2,1)S(1)}, bf16[4,64,1408]{2,1,0:T(8,128)(2,1)S(1)}, u32[]{:S(2)}, u32[]{:S(2)}) %collective-permute-start.29) | collective-permute-done | bytes 720928 | tf_op jit(solution)/shard_map/ppermute | solution.py:59
  149.1 2.6 %collective-permute-done.20.refs_2_ = bf16[64,2048]{1,0:T(8,128)(2,1)S(1)} collective-permute-done((bf16[64,2048]{1,0:T(8,128)(2,1)S(1)}, bf16[64,2048]{1,0:T(8,128)(2,1)S(1)}, u32[]{:S(2)}, u32[]{:S(2)}) %collective-permute-start.20) | collective-permute-done | bytes 262176 | tf_op jit(solution)/shard_map/ppermute | solution.py:59
  151.7 4.8 %collective-permute-start.22 = (bf16[64,2048]{1,0:T(8,128)(2,1)S(1)}, bf16[64,2048]{1,0:T(8,128)(2,1)S(1)}, u32[]{:S(2)}, u32[]{:S(2)}) collective-permute-start(bf16[64,2048]{1,0:T(8,128)(2,1)S(1)} %collective-permute-done.20.refs_2_), channel_id=1, source_target_pairs={{0,1},{1,0},{2,3},{3,2},{4,5},{5,4},{6,7},{7,6},{8,9},{9,8},{10,11... | collective-permute-start | bytes 786440 | tf_op jit(solution)/shard_map/ppermute | solution.py:53
  157.7 9.6 %ffn.1 = (bf16[192,2048]{1,0:T(8,128)(2,1)S(1)}, bf16[64,2048]{1,0:T(8,128)(2,1)S(1)}, bf16[128,2048]{1,0:T(8,128)(2,1)S(1)}, bf16[128,2048]{1,0:T(8,128)(2,1)S(1)}) custom-call(bf16[2,64,2048]{2,1,0:T(8,128)(2,1)S(1)} %bitcast.122, bf16[2,64,2048]{2,1,0:T(8,128)(2,1)S(1)} %collective-permute-done.19.refs_1_, ...), custom_call_target="tpu_custom_call" | custom-call | flops 4429185024 | bytes 13631488 | tf_op jit(solution)/shard_map/ffn/pallas_call | solution.py:303
  170.1 5.3 %collective-permute-done.34 = bf16[64,2048]{1,0:T(8,128)(2,1)S(1)} collective-permute-done((bf16[64,2048]{1,0:T(8,128)(2,1)S(1)}, bf16[64,2048]{1,0:T(8,128)(2,1)S(1)}, u32[]{:S(2)}, u32[]{:S(2)}) %collective-permute-start.34) | collective-permute-done | bytes 262176 | tf_op jit(solution)/shard_map/ppermute | solution.py:59
  176.6 7.4 %collective-permute-done.35 = bf16[128,2048]{1,0:T(8,128)(2,1)S(1)} collective-permute-done((bf16[128,2048]{1,0:T(8,128)(2,1)S(1)}, bf16[128,2048]{1,0:T(8,128)(2,1)S(1)}, u32[]{:S(2)}, u32[]{:S(2)}) %collective-permute-start.35) | collective-permute-done | bytes 524320 | tf_op jit(solution)/shard_map/ppermute | solution.py:59
  184.1 4.6 %collective-permute-start.36 = (bf16[64,2048]{1,0:T(8,128)(2,1)S(1)}, bf16[64,2048]{1,0:T(8,128)(2,1)S(1)}, u32[]{:S(2)}, u32[]{:S(2)}) collective-permute-start(bf16[64,2048]{1,0:T(8,128)(2,1)S(1)} %slice.158), channel_id=1, source_target_pairs={{0,1},{1,0},{2,3},{3,2},{4,5},{5,4},{6,7},{7,6},{8,9},{9,8},{10,11... | collective-permute-start | bytes 786440 | tf_op jit(solution)/shard_map/ppermute | solution.py:53
  190.3 9.2 %all_to_all.10 = bf16[8,64,256]{2,1,0:T(8,128)(2,1)S(1)} all-to-all(bf16[8,64,256]{2,1,0:T(8,128)(2,1)S(1)} %bitcast.126), channel_id=1, replica_groups=mesh['z'=8,'x'=4,'y'=4,'c'=2] {'y','c'}, dimensions={0} | all-to-all | bytes 524288 | tf_op jit(solution)/shard_map/all_to_all | solution.py:359
  (135 shorter events, 45.2 us)
Async XLA Ops:
  0.9 16.1 %collective-permute-start.5 = (bf16[64,1472]{1,0:T(8,128)(2,1)S(1)}, bf16[64,1472]{1,0:T(8,128)(2,1)}, u32[]{:S(2)}, u32[]{:S(2)}) collective-permute-start(bf16[64,1472]{1,0:T(8,128)(2,1)S(1)} %pad_maximum_fusion.4), channel_id=1, source_target_pairs={{0,32},{32,64},{64,96},{96,128},{128,160},{160,192},{192,224},{224... | collective-permute-start | bytes 565256 | tf_op jit(solution)/shard_map/ppermute | solution.py:26
  3.5 15.5 %collective-permute-start.8 = (bf16[64,1472]{1,0:T(8,128)(2,1)S(1)}, bf16[64,1472]{1,0:T(8,128)(2,1)}, u32[]{:S(2)}, u32[]{:S(2)}) collective-permute-start(bf16[64,1472]{1,0:T(8,128)(2,1)S(1)} %pad_maximum_fusion.4), channel_id=1, source_target_pairs={{0,224},{32,0},{64,32},{96,64},{128,96},{160,128},{192,160},{224,1... | collective-permute-start | bytes 565256 | tf_op jit(solution)/shard_map/ppermute | solution.py:26
  9.2 13.3 %collective-permute-start = (bf16[528,256]{1,0:T(8,128)(2,1)S(1)}, bf16[528,256]{1,0:T(8,128)(2,1)S(1)}, u32[]{:S(2)}, u32[]{:S(2)}) collective-permute-start(bf16[528,256]{1,0:T(8,128)(2,1)S(1)} %get-tuple-element.40), channel_id=1, source_target_pairs={{0,1},{1,0},{2,3},{3,2},{4,5},{5,4},{6,7},{7,6},{8,9},{9,8},{10,11... | collective-permute-start | bytes 811016 | tf_op jit(solution)/shard_map/ppermute | solution.py:53
  12.2 19.3 %all-to-all-start = ((bf16[4,64,1408]{2,1,0:T(8,128)(2,1)}), bf16[4,64,1408]{2,1,0:T(8,128)(2,1)S(1)}, u32[]{:S(2)}, u32[]{:S(2)}) async-start(bf16[4,64,1408]{2,1,0:T(8,128)(2,1)} %broadcast_in_dim.83), calls=%async_computation | async-start | bytes 1441792 | tf_op jit(solution)/shard_map/all_to_all | solution.py:338
  18.9 8.1 %collective-permute-start.6 = (bf16[64,1472]{1,0:T(8,128)(2,1)}, bf16[64,1472]{1,0:T(8,128)(2,1)}, u32[]{:S(2)}, u32[]{:S(2)}) collective-permute-start(bf16[64,1472]{1,0:T(8,128)(2,1)} %collective-permute-done.5), channel_id=1, source_target_pairs={{0,32},{32,64},{64,96},{96,128},{128,160},{160,192},{192,224},{224... | collective-permute-start | bytes 565256 | tf_op jit(solution)/shard_map/ppermute | solution.py:26
  19.0 8.1 %collective-permute-start.9 = (bf16[64,1472]{1,0:T(8,128)(2,1)}, bf16[64,1472]{1,0:T(8,128)(2,1)}, u32[]{:S(2)}, u32[]{:S(2)}) collective-permute-start(bf16[64,1472]{1,0:T(8,128)(2,1)} %collective-permute-done.8), channel_id=1, source_target_pairs={{0,224},{32,0},{64,32},{96,64},{128,96},{160,128},{192,160},{224,1... | collective-permute-start | bytes 565256 | tf_op jit(solution)/shard_map/ppermute | solution.py:26
  24.2 36.4 %collective-permute-start.1 = (bf16[2,528,256]{2,1,0:T(8,128)(2,1)S(1)}, bf16[2,528,256]{2,1,0:T(8,128)(2,1)S(1)}, u32[]{:S(2)}, u32[]{:S(2)}) collective-permute-start(bf16[2,528,256]{2,1,0:T(8,128)(2,1)S(1)} %pad_maximum_fusion.refs_0_), channel_id=1, source_target_pairs={{0,2},{2,4},{4,6},{6,0},{1,7},{3,1},{5,3},{7,5},{8,10},{10,12},{12... | collective-permute-start | bytes 1622024 | tf_op jit(solution)/shard_map/ppermute | solution.py:59
  27.1 7.3 %collective-permute-start.7 = (bf16[64,1472]{1,0:T(8,128)(2,1)}, bf16[64,1472]{1,0:T(8,128)(2,1)}, u32[]{:S(2)}, u32[]{:S(2)}) collective-permute-start(bf16[64,1472]{1,0:T(8,128)(2,1)} %collective-permute-done.6), channel_id=1, source_target_pairs={{0,32},{32,64},{64,96},{96,128},{128,160},{160,192},{192,224},{224... | collective-permute-start | bytes 565256 | tf_op jit(solution)/shard_map/ppermute | solution.py:26
  27.1 7.3 %collective-permute-start.10 = (bf16[64,1472]{1,0:T(8,128)(2,1)}, bf16[64,1472]{1,0:T(8,128)(2,1)}, u32[]{:S(2)}, u32[]{:S(2)}) collective-permute-start(bf16[64,1472]{1,0:T(8,128)(2,1)} %collective-permute-done.9), channel_id=1, source_target_pairs={{0,224},{32,0},{64,32},{96,64},{128,96},{160,128},{192,160},{224,1... | collective-permute-start | bytes 565256 | tf_op jit(solution)/shard_map/ppermute | solution.py:26
  31.5 29.4 %collective-permute-start.23 = (bf16[4,64,1408]{2,1,0:T(8,128)(2,1)S(1)}, bf16[4,64,1408]{2,1,0:T(8,128)(2,1)S(1)}, u32[]{:S(2)}, u32[]{:S(2)}) collective-permute-start(bf16[4,64,1408]{2,1,0:T(8,128)(2,1)S(1)} %all-to-all-done), channel_id=1, source_target_pairs={{0,32},{32,64},{64,96},{96,128},{128,160},{160,192},{192,224},{224... | collective-permute-start | bytes 2162696 | tf_op jit(solution)/shard_map/ppermute | solution.py:26
  31.6 53.9 %collective-permute-start.26 = (bf16[4,64,1408]{2,1,0:T(8,128)(2,1)S(1)}, bf16[4,64,1408]{2,1,0:T(8,128)(2,1)S(1)}, u32[]{:S(2)}, u32[]{:S(2)}) collective-permute-start(bf16[4,64,1408]{2,1,0:T(8,128)(2,1)S(1)} %all-to-all-done), channel_id=1, source_target_pairs={{0,224},{32,0},{64,32},{96,64},{128,96},{160,128},{192,160},{224,1... | collective-permute-start | bytes 2162696 | tf_op jit(solution)/shard_map/ppermute | solution.py:26
  35.3 17.2 %collective-permute-start.11 = (bf16[64,1472]{1,0:T(8,128)(2,1)S(1)}, bf16[64,1472]{1,0:T(8,128)(2,1)S(1)}, u32[]{:S(2)}, u32[]{:S(2)}) collective-permute-start(bf16[64,1472]{1,0:T(8,128)(2,1)S(1)} %broadcast_select_fusion.3), channel_id=1, source_target_pairs={{0,32},{32,64},{64,96},{96,128},{128,160},{160,192},{192,224},{224... | collective-permute-start | bytes 565256 | tf_op jit(solution)/shard_map/ppermute | solution.py:59
  55.1 19.3 %collective-permute-start.12 = (bf16[8,64,768]{2,1,0:T(8,128)(2,1)S(1)}, bf16[8,64,768]{2,1,0:T(8,128)(2,1)S(1)}, u32[]{:S(2)}, u32[]{:S(2)}) collective-permute-start(bf16[8,64,768]{2,1,0:T(8,128)(2,1)S(1)} %fusion.16.refs_5_), channel_id=1, source_target_pairs={{0,8},{8,16},{16,24},{24,0},{1,9},{9,17},{17,25},{25,1},{2,10},{10... | collective-permute-start | bytes 2359304 | tf_op jit(solution)/shard_map/ppermute | solution.py:26
  56.6 19.3 %collective-permute-start.13 = (bf16[8,64,768]{2,1,0:T(8,128)(2,1)S(1)}, bf16[8,64,768]{2,1,0:T(8,128)(2,1)S(1)}, u32[]{:S(2)}, u32[]{:S(2)}) collective-permute-start(bf16[8,64,768]{2,1,0:T(8,128)(2,1)S(1)} %fusion.16.refs_5_), channel_id=1, source_target_pairs={{0,24},{8,0},{16,8},{24,16},{1,25},{9,1},{17,9},{25,17},{2,26},{10... | collective-permute-start | bytes 2359304 | tf_op jit(solution)/shard_map/ppermute | solution.py:26
  60.6 30.6 %collective-permute-start.30 = (bf16[8,64,704]{2,1,0:T(8,128)(2,1)S(1)}, bf16[8,64,704]{2,1,0:T(8,128)(2,1)S(1)}, u32[]{:S(2)}, u32[]{:S(2)}) collective-permute-start(bf16[8,64,704]{2,1,0:T(8,128)(2,1)S(1)} %fusion.9), channel_id=1, source_target_pairs={{0,8},{8,16},{16,24},{24,0},{1,9},{9,17},{17,25},{25,1},{2,10},{10... | collective-permute-start | bytes 2162696 | tf_op jit(solution)/shard_map/ppermute | solution.py:26
  60.9 31.7 %collective-permute-start.31 = (bf16[8,64,704]{2,1,0:T(8,128)(2,1)S(1)}, bf16[8,64,704]{2,1,0:T(8,128)(2,1)S(1)}, u32[]{:S(2)}, u32[]{:S(2)}) collective-permute-start(bf16[8,64,704]{2,1,0:T(8,128)(2,1)S(1)} %fusion.9), channel_id=1, source_target_pairs={{0,24},{8,0},{16,8},{24,16},{1,25},{9,1},{17,9},{25,17},{2,26},{10... | collective-permute-start | bytes 2162696 | tf_op jit(solution)/shard_map/ppermute | solution.py:26
  76.0 25.5 %collective-permute-start.14 = (bf16[8,64,768]{2,1,0:T(8,128)(2,1)S(1)}, bf16[8,64,768]{2,1,0:T(8,128)(2,1)S(1)}, u32[]{:S(2)}, u32[]{:S(2)}) collective-permute-start(bf16[8,64,768]{2,1,0:T(8,128)(2,1)S(1)} %broadcast_select_fusion.1), channel_id=1, source_target_pairs={{0,8},{8,16},{16,24},{24,0},{1,25},{9,1},{17,9},{25,17},{2,10},{10... | collective-permute-start | bytes 2359304 | tf_op jit(solution)/shard_map/ppermute | solution.py:59
  80.0 16.6 %collective-permute-start.3 = (bf16[2,528,256]{2,1,0:T(8,128)(2,1)S(1)}, bf16[2,528,256]{2,1,0:T(8,128)(2,1)S(1)}, u32[]{:S(2)}, u32[]{:S(2)}) collective-permute-start(bf16[2,528,256]{2,1,0:T(8,128)(2,1)S(1)} %collective-permute-done.1.refs_1_), channel_id=1, source_target_pairs={{0,1},{1,0},{2,3},{3,2},{4,5},{5,4},{6,7},{7,6},{8,9},{9,8},{10,11... | collective-permute-start | bytes 1622024 | tf_op jit(solution)/shard_map/ppermute | solution.py:53
  85.5 12.6 %collective-permute-start.4 = (bf16[528,256]{1,0:T(8,128)(2,1)S(1)}, bf16[528,256]{1,0:T(8,128)(2,1)S(1)}, u32[]{:S(2)}, u32[]{:S(2)}) collective-permute-start(bf16[528,256]{1,0:T(8,128)(2,1)S(1)} %collective-permute-done.2.refs_2_), channel_id=1, source_target_pairs={{0,1},{1,0},{2,3},{3,2},{4,5},{5,4},{6,7},{7,6},{8,9},{9,8},{10,11... | collective-permute-start | bytes 811016 | tf_op jit(solution)/shard_map/ppermute | solution.py:53
  91.2 21.2 %collective-permute-start.24 = (bf16[4,64,1408]{2,1,0:T(8,128)(2,1)S(1)}, bf16[4,64,1408]{2,1,0:T(8,128)(2,1)S(1)}, u32[]{:S(2)}, u32[]{:S(2)}) collective-permute-start(bf16[4,64,1408]{2,1,0:T(8,128)(2,1)S(1)} %collective-permute-done.23), channel_id=1, source_target_pairs={{0,32},{32,64},{64,96},{96,128},{128,160},{160,192},{192,224},{224... | collective-permute-start | bytes 2162696 | tf_op jit(solution)/shard_map/ppermute | solution.py:26
  92.7 19.8 %collective-permute-start.27 = (bf16[4,64,1408]{2,1,0:T(8,128)(2,1)S(1)}, bf16[4,64,1408]{2,1,0:T(8,128)(2,1)S(1)}, u32[]{:S(2)}, u32[]{:S(2)}) collective-permute-start(bf16[4,64,1408]{2,1,0:T(8,128)(2,1)S(1)} %collective-permute-done.26), channel_id=1, source_target_pairs={{0,224},{32,0},{64,32},{96,64},{128,96},{160,128},{192,160},{224,1... | collective-permute-start | bytes 2162696 | tf_op jit(solution)/shard_map/ppermute | solution.py:26
  96.6 18.7 %collective-permute-start.32 = (bf16[8,64,704]{2,1,0:T(8,128)(2,1)S(1)}, bf16[8,64,704]{2,1,0:T(8,128)(2,1)S(1)}, u32[]{:S(2)}, u32[]{:S(2)}) collective-permute-start(bf16[8,64,704]{2,1,0:T(8,128)(2,1)S(1)} %broadcast_select_fusion), channel_id=1, source_target_pairs={{0,8},{8,16},{16,24},{24,0},{1,25},{9,1},{17,9},{25,17},{2,10},{10... | collective-permute-start | bytes 2162696 | tf_op jit(solution)/shard_map/ppermute | solution.py:59
  109.4 5.9 %collective-permute-start.15 = (bf16[192,2048]{1,0:T(8,128)(2,1)S(1)}, bf16[192,2048]{1,0:T(8,128)(2,1)S(1)}, u32[]{:S(2)}, u32[]{:S(2)}) collective-permute-start(bf16[192,2048]{1,0:T(8,128)(2,1)S(1)} %get-tuple-element.25), channel_id=1, source_target_pairs={{0,1},{1,0},{2,3},{3,2},{4,5},{5,4},{6,7},{7,6},{8,9},{9,8},{10,11... | collective-permute-start | bytes 2359304 | tf_op jit(solution)/shard_map/ppermute | solution.py:53
  112.4 23.1 %collective-permute-start.25 = (bf16[4,64,1408]{2,1,0:T(8,128)(2,1)S(1)}, bf16[4,64,1408]{2,1,0:T(8,128)(2,1)S(1)}, u32[]{:S(2)}, u32[]{:S(2)}) collective-permute-start(bf16[4,64,1408]{2,1,0:T(8,128)(2,1)S(1)} %collective-permute-done.24), channel_id=1, source_target_pairs={{0,32},{32,64},{64,96},{96,128},{128,160},{160,192},{192,224},{224... | collective-permute-start | bytes 2162696 | tf_op jit(solution)/shard_map/ppermute | solution.py:26
  112.5 23.1 %collective-permute-start.28 = (bf16[4,64,1408]{2,1,0:T(8,128)(2,1)S(1)}, bf16[4,64,1408]{2,1,0:T(8,128)(2,1)S(1)}, u32[]{:S(2)}, u32[]{:S(2)}) collective-permute-start(bf16[4,64,1408]{2,1,0:T(8,128)(2,1)S(1)} %collective-permute-done.27), channel_id=1, source_target_pairs={{0,224},{32,0},{64,32},{96,64},{128,96},{160,128},{192,160},{224,1... | collective-permute-start | bytes 2162696 | tf_op jit(solution)/shard_map/ppermute | solution.py:26
  121.2 9.6 %collective-permute-start.17 = (bf16[128,2048]{1,0:T(8,128)(2,1)S(1)}, bf16[128,2048]{1,0:T(8,128)(2,1)S(1)}, u32[]{:S(2)}, u32[]{:S(2)}) collective-permute-start(bf16[128,2048]{1,0:T(8,128)(2,1)S(1)} %pad_maximum_fusion.1), channel_id=1, source_target_pairs={{0,2},{2,4},{4,6},{6,0},{1,7},{3,1},{5,3},{7,5},{8,10},{10,12},{12... | collective-permute-start | bytes 1572872 | tf_op jit(solution)/shard_map/ppermute | solution.py:59
  131.1 6.0 %collective-permute-start.18 = (bf16[128,2048]{1,0:T(8,128)(2,1)S(1)}, bf16[128,2048]{1,0:T(8,128)(2,1)S(1)}, u32[]{:S(2)}, u32[]{:S(2)}) collective-permute-start(bf16[128,2048]{1,0:T(8,128)(2,1)S(1)} %pad_maximum_fusion.2), channel_id=1, source_target_pairs={{0,1},{1,0},{2,3},{3,2},{4,5},{5,4},{6,7},{7,6},{8,9},{9,8},{10,11... | collective-permute-start | bytes 1572872 | tf_op jit(solution)/shard_map/ppermute | solution.py:53
  135.7 10.5 %collective-permute-start.29 = (bf16[4,64,1408]{2,1,0:T(8,128)(2,1)S(1)}, bf16[4,64,1408]{2,1,0:T(8,128)(2,1)S(1)}, u32[]{:S(2)}, u32[]{:S(2)}) collective-permute-start(bf16[4,64,1408]{2,1,0:T(8,128)(2,1)S(1)} %broadcast_select_fusion.2), channel_id=1, source_target_pairs={{0,32},{32,64},{64,96},{96,128},{128,160},{160,192},{192,224},{224... | collective-permute-start | bytes 2162696 | tf_op jit(solution)/shard_map/ppermute | solution.py:59
  138.0 8.4 %collective-permute-start.19 = (bf16[2,64,2048]{2,1,0:T(8,128)(2,1)S(1)}, bf16[2,64,2048]{2,1,0:T(8,128)(2,1)S(1)}, u32[]{:S(2)}, u32[]{:S(2)}) collective-permute-start(bf16[2,64,2048]{2,1,0:T(8,128)(2,1)S(1)} %bitcast.121), channel_id=1, source_target_pairs={{0,2},{2,4},{4,6},{6,0},{1,7},{3,1},{5,3},{7,5},{8,10},{10,12},{12... | collective-permute-start | bytes 1572872 | tf_op jit(solution)/shard_map/ppermute | solution.py:59
  147.7 9.0 %collective-permute-start.21 = (bf16[2,64,2048]{2,1,0:T(8,128)(2,1)S(1)}, bf16[2,64,2048]{2,1,0:T(8,128)(2,1)S(1)}, u32[]{:S(2)}, u32[]{:S(2)}) collective-permute-start(bf16[2,64,2048]{2,1,0:T(8,128)(2,1)S(1)} %collective-permute-done.19.refs_1_), channel_id=1, source_target_pairs={{0,1},{1,0},{2,3},{3,2},{4,5},{5,4},{6,7},{7,6},{8,9},{9,8},{10,11... | collective-permute-start | bytes 1572872 | tf_op jit(solution)/shard_map/ppermute | solution.py:53
  151.7 6.0 %collective-permute-start.22 = (bf16[64,2048]{1,0:T(8,128)(2,1)S(1)}, bf16[64,2048]{1,0:T(8,128)(2,1)S(1)}, u32[]{:S(2)}, u32[]{:S(2)}) collective-permute-start(bf16[64,2048]{1,0:T(8,128)(2,1)S(1)} %collective-permute-done.20.refs_2_), channel_id=1, source_target_pairs={{0,1},{1,0},{2,3},{3,2},{4,5},{5,4},{6,7},{7,6},{8,9},{9,8},{10,11... | collective-permute-start | bytes 786440 | tf_op jit(solution)/shard_map/ppermute | solution.py:53
  175.6 8.4 %collective-permute-start.35 = (bf16[128,2048]{1,0:T(8,128)(2,1)S(1)}, bf16[128,2048]{1,0:T(8,128)(2,1)S(1)}, u32[]{:S(2)}, u32[]{:S(2)}) collective-permute-start(bf16[128,2048]{1,0:T(8,128)(2,1)S(1)} %pad_maximum_fusion.3), channel_id=1, source_target_pairs={{0,2},{2,4},{4,6},{6,0},{1,7},{3,1},{5,3},{7,5},{8,10},{10,12},{12... | collective-permute-start | bytes 1572872 | tf_op jit(solution)/shard_map/ppermute | solution.py:59
  (13 other events, 244.5 us)
where the time goes:
time: 201 us; the launch traced here: 200 us
  waiting for transfers between devices  75.3 us (37%)
  starting transfers between devices  72.1 us (36%)
  Pallas kernels  17.5 us (9%)
  local copies, waits for them, and re-layouts  16.4 us (8%)
  blocking collectives  9.25 us (5%)
  other arithmetic  9.21 us (5%)
    ppermute x12, waiting for transfers between devices, spread(): return lax.ppermute(value, (axis, 'c'), pairs)  51.6 us
    ppermute x16, starting transfers between devices, moved(): return lax.ppermute(value, axis, [(i, (i + by) % n) for i in range(n)])  27.9 us
    ppermute x9, starting transfers between devices, swapped(): return lax.ppermute(value, 'c', [(0, 1), (1, 0)])  22.5 us
    ppermute x16, waiting for transfers between devices, moved(): return lax.ppermute(value, axis, [(i, (i + by) % n) for i in range(n)])  18.4 us
    ppermute x12, starting transfers between devices, spread(): return lax.ppermute(value, (axis, 'c'), pairs)  17.7 us
    pallas_call x1, Pallas kernels, ffn(): pl.pallas_call(ffn_kernel, out_shape=PARTS, in_specs=[VMEM] * 8, out_spec...  9.57 us
    all_to_all x1, blocking collectives, shards(): return lax.all_to_all(to_columns, TP, 0, 0, tiled=True).reshape(ROWS, PIECE)  9.25 us
    pallas_call x1, Pallas kernels, mixer(): pl.pallas_call(mixer_kernel, out_shape=(*PARTS, PAIR, jax.ShapeDtypeStruc...  7.93 us
  transfers between devices with their start and end apart: 38, of which 16 were waited for; matrix products, arithmetic and copies ran while one was open for 11% of the time, Pallas kernels for 4%

commit v1 on v0

--- a/solution.py
+++ b/solution.py
@@ -42,7 +42,8 @@
     n, me = len(blocks), lax.axis_index(axis)
     shape = blocks[0].shape
     whole = jnp.zeros((*shape[:dim], n, *shape[dim:]), blocks[0].dtype)
-    for k in [1, 0, *range(2, n)]:
+    order = [k for j in range(1, n // 2) for k in (j, n - j)] + [n // 2]
+    for k in [1, 0, *order[1:]]:
         start = [0] * whole.ndim
         start[dim] = lax.rem(me + (n - k), n)
         whole = lax.dynamic_update_slice(whole, jnp.expand_dims(blocks[k], dim), start)
@@ -141,11 +142,33 @@
     return lax.rem(me + (n - by), n)
 
 
+def laid_kernel(*refs):
+    blocks, mix_ref, down_ref = refs[:NZ], refs[NZ], refs[NZ + 1]
+    mz = lax.axis_index("z")
+    for k in range(NZ):
+        mix_ref[k] = blocks[k][:, 0:768]
+        down_ref[behind(mz, k, NZ)] = blocks[k][:, 768:]
+
+
+def laid(blocks):
+    return pl.pallas_call(
+        laid_kernel,
+        out_shape=(
+            jax.ShapeDtypeStruct((NZ, 64, 768), bf16), jax.ShapeDtypeStruct((NZ, 64, UNITS), bf16),
+        ),
+        in_specs=[VMEM] * NZ,
+        out_specs=(VMEM,) * 2,
+        compiler_params=pltpu.CompilerParams(vmem_limit_bytes=4 * 1024 * 1024),
+        cost_estimate=pl.CostEstimate(flops=1000, bytes_accessed=3 * 1024 * 1024, transcendentals=0),
+        name="laid",
+    )(*blocks)
+
+
 def mixer_kernel(*refs):
-    x_refs, w_refs = refs[0:5], refs[5:9]
-    taps_ref, recur_ref, inject_ref, slope_ref = refs[9:13]
-    outs, own_ref, gain_ref = refs[13:17], refs[17], refs[18]
-    v_ref, win_ref, wout_ref, gate_ref, in_ref, keep_ref, drive_ref, hid_ref, turned_ref = refs[19:]
+    x_refs, w_refs = [*refs[0:4], refs[3].at[2]], refs[4:8]
+    taps_ref, recur_ref, inject_ref, slope_ref = refs[8:12]
+    outs, own_ref, gain_ref = refs[12:16], refs[16], refs[17]
+    v_ref, win_ref, wout_ref, gate_ref, in_ref, keep_ref, drive_ref, hid_ref, turned_ref = refs[18:]
     mz, mx = lax.axis_index("z"), lax.axis_index("x")
 
     def placed(kz, _):
@@ -169,8 +192,8 @@
         gain_ref[:, at] = ref[ROWS : ROWS + 8, :]
 
     def normed(i, _):
-        rows = stretch(i, 64)
-        squares = jnp.zeros((64, 1), f32)
+        rows = stretch(i, 128)
+        squares = jnp.zeros((128, 1), f32)
         for ref, _at in xs:
             v = ref[rows, :].astype(f32)
             squares = squares + jnp.sum(v * v, axis=1, keepdims=True)
@@ -180,7 +203,7 @@
             v_ref[rows, at] = (ref[rows, :].astype(f32) * factor * gain).astype(bf16)
         return 0
 
-    lax.fori_loop(0, ROWS // 64, normed, 0)
+    lax.fori_loop(0, ROWS // 128, normed, 0)
     gate_ref[...] = jnp.dot(
         v_ref[...], win_ref[:, 0:PIECE], preferred_element_type=f32
     ).astype(bf16)
@@ -222,7 +245,7 @@
     projected(hid_ref, turned_ref, wout_ref, outs)
 
 
-CHUNK = 128
+CHUNK = 256
 TOP = 16
 VMEM = pl.BlockSpec(memory_space=pltpu.VMEM)
 PARTS = tuple(jax.ShapeDtypeStruct((n * OWN, D), bf16) for n in (3, 1, 2, 2))
@@ -246,7 +269,7 @@
             pltpu.VMEM((ROWS, PIECE), bf16),
             pltpu.VMEM((ROWS, PIECE), bf16),
         ],
-        compiler_params=pltpu.CompilerParams(vmem_limit_bytes=24 * 1024 * 1024),
+        compiler_params=pltpu.CompilerParams(vmem_limit_bytes=14 * 1024 * 1024),
         cost_estimate=pl.CostEstimate(
             flops=2 * ROWS * D * 768 + 4 * ROWS * PIECE * PIECE,
             bytes_accessed=8 * 1024 * 1024, transcendentals=ROWS * PIECE * 6,
@@ -311,7 +334,7 @@
             pltpu.VMEM((ROWS, UNITS), bf16),
             pltpu.VMEM((ROWS, UNITS), bf16),
         ],
-        compiler_params=pltpu.CompilerParams(vmem_limit_bytes=28 * 1024 * 1024),
+        compiler_params=pltpu.CompilerParams(vmem_limit_bytes=14 * 1024 * 1024),
         cost_estimate=pl.CostEstimate(
             flops=2 * ROWS * D * 3 * UNITS, bytes_accessed=13 * 1024 * 1024,
             transcendentals=ROWS * UNITS,
@@ -330,14 +353,15 @@
     gains = jnp.concatenate([pre_mix_gain, post_mix_gain, pre_ffn_gain, post_ffn_gain])
     gains = gains.reshape(4, PIECE)
     packed = jnp.concatenate([tokens, jnp.pad(gains, ((0, EXTRA - 4), (0, 0)))], axis=0)
-    mix_blocks = ring_gathered(jnp.stack([b[:, :768] for b in along_z]), "x", NX)
+    mix_z, down_z = laid(along_z)
+    mix_blocks = ring_gathered(mix_z, "x", NX)
     packed = jnp.stack([packed, swapped(packed)])
-    x_blocks = rows_ring(packed)
+    p, far = ring_pieces(packed, "y", NY)
+    x_blocks = [*p, far, swapped(jnp.concatenate([p[1], far[None]], axis=0))]
     up_own = jnp.concatenate([w_up_gate, w_up_value], axis=1)
     sent = jnp.broadcast_to(up_own[None], (NX, *up_own.shape))
     along_x = lax.all_to_all(sent, "x", 0, 0, tiled=True)
     up_all = in_order(ring_gathered(along_x, "z", NZ), "z", 0).reshape(D, 2 * UNITS)
-    down_z = in_order([b[:, 768:] for b in along_z], "z", 0)
     down_all = in_order(ring_gathered(down_z, "x", NX), "x", 1).reshape(D, UNITS)
     x_blocks[1], decay_param = lax.optimization_barrier((x_blocks[1], decay_param))
     slope = jax.nn.softplus(-decay_param)[None, :]

time: 201 us -> 182 us (0.905)
  waiting for transfers between devices: 75.3 us -> 63.9 us
  local copies, waits for them, and re-layouts: 16.4 us -> 6.15 us
  starting transfers between devices: 72.1 us -> 78.5 us
  other arithmetic: 9.21 us -> 6.58 us
    ppermute x9 -> x8, starting transfers between devices: 22.5 us -> 34.1 us  [swapped(): return lax.ppermute(value, 'c', [(0, 1), (1, 0)])]
    ppermute x16, waiting for transfers between devices: 18.4 us -> 10.2 us  [moved(): return lax.ppermute(value, axis, [(i, (i + by) % n) for i in range(n)])]
    unnamed x21 -> x13, local copies, waits for them, and re-layouts: 5.94 us -> 0.74 us
    dynamic_update_slice x20 -> x12, local copies, waits for them, and re-layouts: 7.3 us -> 3.25 us  [in_order(): lax.dynamic_update_slice(whole, jnp.expand_dims(blocks[k], dim), start)]
    ppermute x12, waiting for transfers between devices: 51.6 us -> 48.2 us  [spread(): return lax.ppermute(value, (axis, 'c'), pairs)]
    ppermute x16, starting transfers between devices: 27.9 us -> 24.9 us  [moved(): return lax.ppermute(value, axis, [(i, (i + by) % n) for i in range(n)])]
    ppermute x12, starting transfers between devices: 17.7 us -> 15.3 us  [spread(): return lax.ppermute(value, (axis, 'c'), pairs)]
    ppermute x9 -> x8, waiting for transfers between devices: 5.26 us -> 5.46 us  [swapped(): return lax.ppermute(value, 'c', [(0, 1), (1, 0)])]
  transfers between devices with their start and end apart: 38 -> 37, of which waited for: 16 -> 16; matrix products, arithmetic and copies ran while one was open for 11% -> 6% of each run, Pallas kernels for 4% -> 4%
where the time goes in v1:
time: 182 us
  starting transfers between devices  78.5 us (43%)
  waiting for transfers between devices  63.9 us (35%)
  Pallas kernels  17.1 us (9%)
  blocking collectives  9.25 us (5%)
  other arithmetic  6.58 us (4%)
  local copies, waits for them, and re-layouts  6.15 us (3%)
    ppermute x12, waiting for transfers between devices, spread(): return lax.ppermute(value, (axis, 'c'), pairs)  48.2 us
    ppermute x8, starting transfers between devices, swapped(): return lax.ppermute(value, 'c', [(0, 1), (1, 0)])  34.1 us
    ppermute x16, starting transfers between devices, moved(): return lax.ppermute(value, axis, [(i, (i + by) % n) for i in range(n)])  24.9 us
    ppermute x12, starting transfers between devices, spread(): return lax.ppermute(value, (axis, 'c'), pairs)  15.3 us
    ppermute x16, waiting for transfers between devices, moved(): return lax.ppermute(value, axis, [(i, (i + by) % n) for i in range(n)])  10.2 us
    pallas_call x1, Pallas kernels, ffn(): pl.pallas_call(ffn_kernel, out_shape=PARTS, in_specs=[VMEM] * 8, out_spec...  9.57 us
    all_to_all x1, blocking collectives, shards(): return lax.all_to_all(to_columns, TP, 0, 0, tiled=True).reshape(ROWS, PIECE)  9.25 us
    pallas_call x1, Pallas kernels, mixer(): pl.pallas_call(mixer_kernel, out_shape=(*PARTS, PAIR, jax.ShapeDtypeStruc...  7.4 us
  transfers between devices with their start and end apart: 37, of which 16 were waited for; matrix products, arithmetic and copies ran while one was open for 6% of the time, Pallas kernels for 4%

profile of v1, /device:TPU:1, one launch (start us, length us, event | category | flops | bytes accessed | tf_op | source)
XLA Modules:
  0.0 182.0 jit_solution(15804142886601554700)
XLA Ops:
  0.9 2.5 %collective-permute-start.4 = (bf16[64,1472]{1,0:T(8,128)(2,1)S(1)}, bf16[64,1472]{1,0:T(8,128)(2,1)S(1)}, u32[]{:S(2)}, u32[]{:S(2)}) collective-permute-start(bf16[64,1472]{1,0:T(8,128)(2,1)S(1)} %pad_maximum_fusion.5.refs_0_), channel_id=1, source_target_pairs={{0,32},{32,64},{64,96},{96,128},{128,160},{160,192},{192,224},{224... | collective-permute-start | bytes 565256 | tf_op jit(solution)/shard_map/ppermute | solution.py:26
  3.5 4.0 %collective-permute-start.7 = (bf16[64,1472]{1,0:T(8,128)(2,1)S(1)}, bf16[64,1472]{1,0:T(8,128)(2,1)S(1)}, u32[]{:S(2)}, u32[]{:S(2)}) collective-permute-start(bf16[64,1472]{1,0:T(8,128)(2,1)S(1)} %pad_maximum_fusion.5.refs_0_), channel_id=1, source_target_pairs={{0,224},{32,0},{64,32},{96,64},{128,96},{160,128},{192,160},{224,1... | collective-permute-start | bytes 565256 | tf_op jit(solution)/shard_map/ppermute | solution.py:26
  9.5 4.2 %all-to-all-start = ((bf16[4,64,1408]{2,1,0:T(8,128)(2,1)}), bf16[4,64,1408]{2,1,0:T(8,128)(2,1)}, u32[]{:S(2)}, u32[]{:S(2)}) async-start(bf16[4,64,1408]{2,1,0:T(8,128)(2,1)} %broadcast_in_dim.60), calls=%async_computation | async-start | bytes 1441792 | tf_op jit(solution)/shard_map/all_to_all | solution.py:363
  16.5 2.7 %collective-permute-start.8 = (bf16[64,1472]{1,0:T(8,128)(2,1)S(1)}, bf16[64,1472]{1,0:T(8,128)(2,1)S(1)}, u32[]{:S(2)}, u32[]{:S(2)}) collective-permute-start(bf16[64,1472]{1,0:T(8,128)(2,1)S(1)} %collective-permute-done.7.refs_7_), channel_id=1, source_target_pairs={{0,224},{32,0},{64,32},{96,64},{128,96},{160,128},{192,160},{224,1... | collective-permute-start | bytes 565256 | tf_op jit(solution)/shard_map/ppermute | solution.py:26
  19.2 5.0 %collective-permute-done.5.refs_2_ = bf16[64,1472]{1,0:T(8,128)(2,1)S(1)} collective-permute-done((bf16[64,1472]{1,0:T(8,128)(2,1)S(1)}, bf16[64,1472]{1,0:T(8,128)(2,1)S(1)}, u32[]{:S(2)}, u32[]{:S(2)}) %collective-permute-start.5) | collective-permute-done | bytes 188448 | tf_op jit(solution)/shard_map/ppermute | solution.py:26
  24.2 2.7 %collective-permute-start.9 = (bf16[64,1472]{1,0:T(8,128)(2,1)S(1)}, bf16[64,1472]{1,0:T(8,128)(2,1)S(1)}, u32[]{:S(2)}, u32[]{:S(2)}) collective-permute-start(bf16[64,1472]{1,0:T(8,128)(2,1)S(1)} %collective-permute-done.8.refs_6_), channel_id=1, source_target_pairs={{0,224},{32,0},{64,32},{96,64},{128,96},{160,128},{192,160},{224,1... | collective-permute-start | bytes 565256 | tf_op jit(solution)/shard_map/ppermute | solution.py:26
  26.9 2.8 %collective-permute-start.1 = (bf16[2,528,256]{2,1,0:T(8,128)(2,1)S(1)}, bf16[2,528,256]{2,1,0:T(8,128)(2,1)S(1)}, u32[]{:S(2)}, u32[]{:S(2)}) collective-permute-start(bf16[2,528,256]{2,1,0:T(8,128)(2,1)S(1)} %pad_maximum_fusion.1.refs_0_), channel_id=1, source_target_pairs={{0,2},{2,4},{4,6},{6,0},{1,7},{3,1},{5,3},{7,5},{8,10},{10,12},{12... | collective-permute-start | bytes 1622024 | tf_op jit(solution)/shard_map/ppermute | solution.py:60
  31.0 2.5 %collective-permute-start.10 = (bf16[64,1472]{1,0:T(8,128)(2,1)S(1)}, bf16[64,1472]{1,0:T(8,128)(2,1)S(1)}, u32[]{:S(2)}, u32[]{:S(2)}) collective-permute-start(bf16[64,1472]{1,0:T(8,128)(2,1)S(1)} %broadcast_select_fusion.3), channel_id=1, source_target_pairs={{0,32},{32,64},{64,96},{96,128},{128,160},{160,192},{192,224},{224... | collective-permute-start | bytes 565256 | tf_op jit(solution)/shard_map/ppermute | solution.py:60
  33.5 2.5 %collective-permute-done.1.refs_1_ = bf16[2,528,256]{2,1,0:T(8,128)(2,1)S(1)} collective-permute-done((bf16[2,528,256]{2,1,0:T(8,128)(2,1)S(1)}, bf16[2,528,256]{2,1,0:T(8,128)(2,1)S(1)}, u32[]{:S(2)}, u32[]{:S(2)}) %collective-permute-start.1) | collective-permute-done | bytes 540704 | tf_op jit(solution)/shard_map/ppermute | solution.py:60
  36.1 3.6 %collective-permute-start.2 = (bf16[528,256]{1,0:T(8,128)(2,1)S(1)}, bf16[528,256]{1,0:T(8,128)(2,1)S(1)}, u32[]{:S(2)}, u32[]{:S(2)}) collective-permute-start(bf16[528,256]{1,0:T(8,128)(2,1)S(1)} %slice_bitcast_fusion), channel_id=1, source_target_pairs={{0,2},{2,4},{4,6},{6,0},{1,7},{3,1},{5,3},{7,5},{8,10},{10,12},{12... | collective-permute-start | bytes 811016 | tf_op jit(solution)/shard_map/ppermute | solution.py:60
  39.8 1.7 collective-permute-start.11
  43.1 1.6 collective-permute-start.29
  44.8 3.9 %collective-permute-done.22 = bf16[4,64,1408]{2,1,0:T(8,128)(2,1)} collective-permute-done((bf16[4,64,1408]{2,1,0:T(8,128)(2,1)}, bf16[4,64,1408]{2,1,0:T(8,128)(2,1)}, u32[]{:S(2)}, u32[]{:S(2)}) %collective-permute-start.22) | collective-permute-done | bytes 720928 | tf_op jit(solution)/shard_map/ppermute | solution.py:26
  48.7 2.7 %collective-permute-start.30 = (bf16[8,64,704]{2,1,0:T(8,128)(2,1)S(1)}, bf16[8,64,704]{2,1,0:T(8,128)(2,1)S(1)}, u32[]{:S(2)}, u32[]{:S(2)}) collective-permute-start(bf16[8,64,704]{2,1,0:T(8,128)(2,1)S(1)} %get-tuple-element.32), channel_id=1, source_target_pairs={{0,24},{8,0},{16,8},{24,16},{1,25},{9,1},{17,9},{25,17},{2,26},{10... | collective-permute-start | bytes 2162696 | tf_op jit(solution)/shard_map/ppermute | solution.py:26
  53.5 16.2 %collective-permute-start.3 = (bf16[3,528,256]{2,1,0:T(8,128)(2,1)S(1)}, bf16[3,528,256]{2,1,0:T(8,128)(2,1)S(1)}, u32[]{:S(2)}, u32[]{:S(2)}) collective-permute-start(bf16[3,528,256]{2,1,0:T(8,128)(2,1)S(1)} %pad_maximum_fusion), channel_id=1, source_target_pairs={{0,1},{1,0},{2,3},{3,2},{4,5},{5,4},{6,7},{7,6},{8,9},{9,8},{10,11... | collective-permute-start | bytes 2433032 | tf_op jit(solution)/shard_map/ppermute | solution.py:54
  69.7 1.5 collective-permute-start.13
  72.5 1.5 collective-permute-start.24
  76.2 10.2 %collective-permute-done.13.refs_6_ = bf16[8,64,768]{2,1,0:T(8,128)(2,1)S(1)} collective-permute-done((bf16[8,64,768]{2,1,0:T(8,128)(2,1)S(1)}, bf16[8,64,768]{2,1,0:T(8,128)(2,1)S(1)}, u32[]{:S(2)}, u32[]{:S(2)}) %collective-permute-start.13) | collective-permute-done | bytes 786464 | tf_op jit(solution)/shard_map/ppermute | solution.py:60
  86.4 7.4 %mixer.1 = (bf16[192,2048]{1,0:T(8,128)(2,1)S(1)}, bf16[64,2048]{1,0:T(8,128)(2,1)S(1)}, bf16[128,2048]{1,0:T(8,128)(2,1)S(1)}, bf16[128,2048]{1,0:T(8,128)(2,1)...) custom-call(bf16[2,528,256]{2,1,0:T(8,128)(2,1)S(1)} %pad_maximum_fusion.1.refs_0_, ...), custom_call_target="tpu_custom_call" | custom-call | flops 1744830464 | bytes 8388608 | tf_op jit(solution)/shard_map/mixer/pallas_call | solution.py:256
  94.6 1.5 collective-permute-start.26
  98.0 5.2 %collective-permute-done.15 = bf16[64,2048]{1,0:T(8,128)(2,1)S(1)} collective-permute-done((bf16[64,2048]{1,0:T(8,128)(2,1)S(1)}, bf16[64,2048]{1,0:T(8,128)(2,1)S(1)}, u32[]{:S(2)}, u32[]{:S(2)}) %collective-permute-start.15) | collective-permute-done | bytes 262176 | tf_op jit(solution)/shard_map/ppermute | solution.py:60
  105.0 6.7 %collective-permute-done.16 = bf16[128,2048]{1,0:T(8,128)(2,1)S(1)} collective-permute-done((bf16[128,2048]{1,0:T(8,128)(2,1)S(1)}, bf16[128,2048]{1,0:T(8,128)(2,1)S(1)}, u32[]{:S(2)}, u32[]{:S(2)}) %collective-permute-start.16) | collective-permute-done | bytes 524320 | tf_op jit(solution)/shard_map/ppermute | solution.py:60
  111.9 5.3 %collective-permute-start.17 = (bf16[128,2048]{1,0:T(8,128)(2,1)S(1)}, bf16[128,2048]{1,0:T(8,128)(2,1)S(1)}, u32[]{:S(2)}, u32[]{:S(2)}) collective-permute-start(bf16[128,2048]{1,0:T(8,128)(2,1)S(1)} %pad_maximum_fusion.3), channel_id=1, source_target_pairs={{0,1},{1,0},{2,3},{3,2},{4,5},{5,4},{6,7},{7,6},{8,9},{9,8},{10,11... | collective-permute-start | bytes 1572872 | tf_op jit(solution)/shard_map/ppermute | solution.py:54
  120.2 8.0 %collective-permute-done.18.refs_1_ = bf16[2,64,2048]{2,1,0:T(8,128)(2,1)S(1)} collective-permute-done((bf16[2,64,2048]{2,1,0:T(8,128)(2,1)S(1)}, bf16[2,64,2048]{2,1,0:T(8,128)(2,1)S(1)}, u32[]{:S(2)}, u32[]{:S(2)}) %collective-permute-start.18) | collective-permute-done | bytes 524320 | tf_op jit(solution)/shard_map/ppermute | solution.py:60
  130.9 2.6 %collective-permute-done.19.refs_2_ = bf16[64,2048]{1,0:T(8,128)(2,1)S(1)} collective-permute-done((bf16[64,2048]{1,0:T(8,128)(2,1)S(1)}, bf16[64,2048]{1,0:T(8,128)(2,1)S(1)}, u32[]{:S(2)}, u32[]{:S(2)}) %collective-permute-start.19) | collective-permute-done | bytes 262176 | tf_op jit(solution)/shard_map/ppermute | solution.py:60
  133.5 4.8 %collective-permute-start.21 = (bf16[64,2048]{1,0:T(8,128)(2,1)S(1)}, bf16[64,2048]{1,0:T(8,128)(2,1)S(1)}, u32[]{:S(2)}, u32[]{:S(2)}) collective-permute-start(bf16[64,2048]{1,0:T(8,128)(2,1)S(1)} %collective-permute-done.19.refs_2_), channel_id=1, source_target_pairs={{0,1},{1,0},{2,3},{3,2},{4,5},{5,4},{6,7},{7,6},{8,9},{9,8},{10,11... | collective-permute-start | bytes 786440 | tf_op jit(solution)/shard_map/ppermute | solution.py:54
  139.4 9.6 %ffn.1 = (bf16[192,2048]{1,0:T(8,128)(2,1)S(1)}, bf16[64,2048]{1,0:T(8,128)(2,1)S(1)}, bf16[128,2048]{1,0:T(8,128)(2,1)S(1)}, bf16[128,2048]{1,0:T(8,128)(2,1)S(1)}) custom-call(bf16[2,64,2048]{2,1,0:T(8,128)(2,1)S(1)} %bitcast.62, bf16[2,64,2048]{2,1,0:T(8,128)(2,1)S(1)} %collective-permute-done.18.refs_1_, ...), custom_call_target="tpu_custom_call" | custom-call | flops 4429185024 | bytes 13631488 | tf_op jit(solution)/shard_map/ffn/pallas_call | solution.py:326
  149.5 1.9 %collective-permute-done.32 = bf16[192,2048]{1,0:T(8,128)(2,1)S(1)} collective-permute-done((bf16[192,2048]{1,0:T(8,128)(2,1)S(1)}, bf16[192,2048]{1,0:T(8,128)(2,1)S(1)}, u32[]{:S(2)}, u32[]{:S(2)}) %collective-permute-start.32) | collective-permute-done | bytes 786464 | tf_op jit(solution)/shard_map/ppermute | solution.py:54
  151.9 5.3 %collective-permute-done.33 = bf16[64,2048]{1,0:T(8,128)(2,1)S(1)} collective-permute-done((bf16[64,2048]{1,0:T(8,128)(2,1)S(1)}, bf16[64,2048]{1,0:T(8,128)(2,1)S(1)}, u32[]{:S(2)}, u32[]{:S(2)}) %collective-permute-start.33) | collective-permute-done | bytes 262176 | tf_op jit(solution)/shard_map/ppermute | solution.py:60
  158.3 7.4 %collective-permute-done.34 = bf16[128,2048]{1,0:T(8,128)(2,1)S(1)} collective-permute-done((bf16[128,2048]{1,0:T(8,128)(2,1)S(1)}, bf16[128,2048]{1,0:T(8,128)(2,1)S(1)}, u32[]{:S(2)}, u32[]{:S(2)}) %collective-permute-start.34) | collective-permute-done | bytes 524320 | tf_op jit(solution)/shard_map/ppermute | solution.py:60
  165.9 4.6 %collective-permute-start.35 = (bf16[64,2048]{1,0:T(8,128)(2,1)S(1)}, bf16[64,2048]{1,0:T(8,128)(2,1)S(1)}, u32[]{:S(2)}, u32[]{:S(2)}) collective-permute-start(bf16[64,2048]{1,0:T(8,128)(2,1)S(1)} %slice.86), channel_id=1, source_target_pairs={{0,1},{1,0},{2,3},{3,2},{4,5},{5,4},{6,7},{7,6},{8,9},{9,8},{10,11... | collective-permute-start | bytes 786440 | tf_op jit(solution)/shard_map/ppermute | solution.py:54
  172.0 9.2 %all_to_all.10 = bf16[8,64,256]{2,1,0:T(8,128)(2,1)S(1)} all-to-all(bf16[8,64,256]{2,1,0:T(8,128)(2,1)S(1)} %bitcast.67), channel_id=1, replica_groups=mesh['z'=8,'x'=4,'y'=4,'c'=2] {'y','c'}, dimensions={0} | all-to-all | bytes 524288 | tf_op jit(solution)/shard_map/all_to_all | solution.py:383
  (116 shorter events, 29.9 us)
Async XLA Ops:
  0.9 15.6 %collective-permute-start.4 = (bf16[64,1472]{1,0:T(8,128)(2,1)S(1)}, bf16[64,1472]{1,0:T(8,128)(2,1)S(1)}, u32[]{:S(2)}, u32[]{:S(2)}) collective-permute-start(bf16[64,1472]{1,0:T(8,128)(2,1)S(1)} %pad_maximum_fusion.5.refs_0_), channel_id=1, source_target_pairs={{0,32},{32,64},{64,96},{96,128},{128,160},{160,192},{192,224},{224... | collective-permute-start | bytes 565256 | tf_op jit(solution)/shard_map/ppermute | solution.py:26
  3.5 13.1 %collective-permute-start.7 = (bf16[64,1472]{1,0:T(8,128)(2,1)S(1)}, bf16[64,1472]{1,0:T(8,128)(2,1)S(1)}, u32[]{:S(2)}, u32[]{:S(2)}) collective-permute-start(bf16[64,1472]{1,0:T(8,128)(2,1)S(1)} %pad_maximum_fusion.5.refs_0_), channel_id=1, source_target_pairs={{0,224},{32,0},{64,32},{96,64},{128,96},{160,128},{192,160},{224,1... | collective-permute-start | bytes 565256 | tf_op jit(solution)/shard_map/ppermute | solution.py:26
  9.5 20.3 %all-to-all-start = ((bf16[4,64,1408]{2,1,0:T(8,128)(2,1)}), bf16[4,64,1408]{2,1,0:T(8,128)(2,1)}, u32[]{:S(2)}, u32[]{:S(2)}) async-start(bf16[4,64,1408]{2,1,0:T(8,128)(2,1)} %broadcast_in_dim.60), calls=%async_computation | async-start | bytes 1441792 | tf_op jit(solution)/shard_map/all_to_all | solution.py:363
  15.4 11.5 %collective-permute-start = (bf16[528,256]{1,0:T(8,128)(2,1)S(1)}, bf16[528,256]{1,0:T(8,128)(2,1)S(1)}, u32[]{:S(2)}, u32[]{:S(2)}) collective-permute-start(bf16[528,256]{1,0:T(8,128)(2,1)S(1)} %get-tuple-element.44), channel_id=1, source_target_pairs={{0,1},{1,0},{2,3},{3,2},{4,5},{5,4},{6,7},{7,6},{8,9},{9,8},{10,11... | collective-permute-start | bytes 811016 | tf_op jit(solution)/shard_map/ppermute | solution.py:54
  16.5 7.7 %collective-permute-start.5 = (bf16[64,1472]{1,0:T(8,128)(2,1)S(1)}, bf16[64,1472]{1,0:T(8,128)(2,1)S(1)}, u32[]{:S(2)}, u32[]{:S(2)}) collective-permute-start(bf16[64,1472]{1,0:T(8,128)(2,1)S(1)} %collective-permute-done.4.refs_1_), channel_id=1, source_target_pairs={{0,32},{32,64},{64,96},{96,128},{128,160},{160,192},{192,224},{224... | collective-permute-start | bytes 565256 | tf_op jit(solution)/shard_map/ppermute | solution.py:26
  16.5 7.7 %collective-permute-start.8 = (bf16[64,1472]{1,0:T(8,128)(2,1)S(1)}, bf16[64,1472]{1,0:T(8,128)(2,1)S(1)}, u32[]{:S(2)}, u32[]{:S(2)}) collective-permute-start(bf16[64,1472]{1,0:T(8,128)(2,1)S(1)} %collective-permute-done.7.refs_7_), channel_id=1, source_target_pairs={{0,224},{32,0},{64,32},{96,64},{128,96},{160,128},{192,160},{224,1... | collective-permute-start | bytes 565256 | tf_op jit(solution)/shard_map/ppermute | solution.py:26
  24.2 6.8 %collective-permute-start.6 = (bf16[64,1472]{1,0:T(8,128)(2,1)S(1)}, bf16[64,1472]{1,0:T(8,128)(2,1)S(1)}, u32[]{:S(2)}, u32[]{:S(2)}) collective-permute-start(bf16[64,1472]{1,0:T(8,128)(2,1)S(1)} %collective-permute-done.5.refs_2_), channel_id=1, source_target_pairs={{0,32},{32,64},{64,96},{96,128},{128,160},{160,192},{192,224},{224... | collective-permute-start | bytes 565256 | tf_op jit(solution)/shard_map/ppermute | solution.py:26
  24.2 6.8 %collective-permute-start.9 = (bf16[64,1472]{1,0:T(8,128)(2,1)S(1)}, bf16[64,1472]{1,0:T(8,128)(2,1)S(1)}, u32[]{:S(2)}, u32[]{:S(2)}) collective-permute-start(bf16[64,1472]{1,0:T(8,128)(2,1)S(1)} %collective-permute-done.8.refs_6_), channel_id=1, source_target_pairs={{0,224},{32,0},{64,32},{96,64},{128,96},{160,128},{192,160},{224,1... | collective-permute-start | bytes 565256 | tf_op jit(solution)/shard_map/ppermute | solution.py:26
  26.9 9.1 %collective-permute-start.1 = (bf16[2,528,256]{2,1,0:T(8,128)(2,1)S(1)}, bf16[2,528,256]{2,1,0:T(8,128)(2,1)S(1)}, u32[]{:S(2)}, u32[]{:S(2)}) collective-permute-start(bf16[2,528,256]{2,1,0:T(8,128)(2,1)S(1)} %pad_maximum_fusion.1.refs_0_), channel_id=1, source_target_pairs={{0,2},{2,4},{4,6},{6,0},{1,7},{3,1},{5,3},{7,5},{8,10},{10,12},{12... | collective-permute-start | bytes 1622024 | tf_op jit(solution)/shard_map/ppermute | solution.py:60
  29.7 19.0 %collective-permute-start.22 = (bf16[4,64,1408]{2,1,0:T(8,128)(2,1)}, bf16[4,64,1408]{2,1,0:T(8,128)(2,1)}, u32[]{:S(2)}, u32[]{:S(2)}) collective-permute-start(bf16[4,64,1408]{2,1,0:T(8,128)(2,1)} %all-to-all-done), channel_id=1, source_target_pairs={{0,32},{32,64},{64,96},{96,128},{128,160},{160,192},{192,224},{224... | collective-permute-start | bytes 2162696 | tf_op jit(solution)/shard_map/ppermute | solution.py:26
  31.0 8.6 %collective-permute-start.10 = (bf16[64,1472]{1,0:T(8,128)(2,1)S(1)}, bf16[64,1472]{1,0:T(8,128)(2,1)S(1)}, u32[]{:S(2)}, u32[]{:S(2)}) collective-permute-start(bf16[64,1472]{1,0:T(8,128)(2,1)S(1)} %broadcast_select_fusion.3), channel_id=1, source_target_pairs={{0,32},{32,64},{64,96},{96,128},{128,160},{160,192},{192,224},{224... | collective-permute-start | bytes 565256 | tf_op jit(solution)/shard_map/ppermute | solution.py:60
  36.1 7.0 %collective-permute-start.2 = (bf16[528,256]{1,0:T(8,128)(2,1)S(1)}, bf16[528,256]{1,0:T(8,128)(2,1)S(1)}, u32[]{:S(2)}, u32[]{:S(2)}) collective-permute-start(bf16[528,256]{1,0:T(8,128)(2,1)S(1)} %slice_bitcast_fusion), channel_id=1, source_target_pairs={{0,2},{2,4},{4,6},{6,0},{1,7},{3,1},{5,3},{7,5},{8,10},{10,12},{12... | collective-permute-start | bytes 811016 | tf_op jit(solution)/shard_map/ppermute | solution.py:60
  39.7 32.8 %collective-permute-start.23 = (bf16[4,64,1408]{2,1,0:T(8,128)(2,1)}, bf16[4,64,1408]{2,1,0:T(8,128)(2,1)S(1)}, u32[]{:S(2)}, u32[]{:S(2)}) collective-permute-start(bf16[4,64,1408]{2,1,0:T(8,128)(2,1)} %all-to-all-done), channel_id=1, source_target_pairs={{0,224},{32,0},{64,32},{96,64},{128,96},{160,128},{192,160},{224,1... | collective-permute-start | bytes 2162696 | tf_op jit(solution)/shard_map/ppermute | solution.py:26
  39.8 13.7 %collective-permute-start.11 = (bf16[8,64,768]{2,1,0:T(8,128)(2,1)S(1)}, bf16[8,64,768]{2,1,0:T(8,128)(2,1)S(1)}, u32[]{:S(2)}, u32[]{:S(2)}) collective-permute-start(bf16[8,64,768]{2,1,0:T(8,128)(2,1)S(1)} %get-tuple-element.23.refs_4_), channel_id=1, source_target_pairs={{0,8},{8,16},{16,24},{24,0},{1,9},{9,17},{17,25},{25,1},{2,10},{10... | collective-permute-start | bytes 2359304 | tf_op jit(solution)/shard_map/ppermute | solution.py:26
  41.5 28.1 %collective-permute-start.12 = (bf16[8,64,768]{2,1,0:T(8,128)(2,1)S(1)}, bf16[8,64,768]{2,1,0:T(8,128)(2,1)S(1)}, u32[]{:S(2)}, u32[]{:S(2)}) collective-permute-start(bf16[8,64,768]{2,1,0:T(8,128)(2,1)S(1)} %get-tuple-element.23.refs_4_), channel_id=1, source_target_pairs={{0,24},{8,0},{16,8},{24,16},{1,25},{9,1},{17,9},{25,17},{2,26},{10... | collective-permute-start | bytes 2359304 | tf_op jit(solution)/shard_map/ppermute | solution.py:26
  43.1 31.1 %collective-permute-start.29 = (bf16[8,64,704]{2,1,0:T(8,128)(2,1)S(1)}, bf16[8,64,704]{2,1,0:T(8,128)(2,1)S(1)}, u32[]{:S(2)}, u32[]{:S(2)}) collective-permute-start(bf16[8,64,704]{2,1,0:T(8,128)(2,1)S(1)} %get-tuple-element.32), channel_id=1, source_target_pairs={{0,8},{8,16},{16,24},{24,0},{1,9},{9,17},{17,25},{25,1},{2,10},{10... | collective-permute-start | bytes 2162696 | tf_op jit(solution)/shard_map/ppermute | solution.py:26
  48.7 26.7 %collective-permute-start.30 = (bf16[8,64,704]{2,1,0:T(8,128)(2,1)S(1)}, bf16[8,64,704]{2,1,0:T(8,128)(2,1)S(1)}, u32[]{:S(2)}, u32[]{:S(2)}) collective-permute-start(bf16[8,64,704]{2,1,0:T(8,128)(2,1)S(1)} %get-tuple-element.32), channel_id=1, source_target_pairs={{0,24},{8,0},{16,8},{24,16},{1,25},{9,1},{17,9},{25,17},{2,26},{10... | collective-permute-start | bytes 2162696 | tf_op jit(solution)/shard_map/ppermute | solution.py:26
  53.5 22.7 %collective-permute-start.3 = (bf16[3,528,256]{2,1,0:T(8,128)(2,1)S(1)}, bf16[3,528,256]{2,1,0:T(8,128)(2,1)S(1)}, u32[]{:S(2)}, u32[]{:S(2)}) collective-permute-start(bf16[3,528,256]{2,1,0:T(8,128)(2,1)S(1)} %pad_maximum_fusion), channel_id=1, source_target_pairs={{0,1},{1,0},{2,3},{3,2},{4,5},{5,4},{6,7},{7,6},{8,9},{9,8},{10,11... | collective-permute-start | bytes 2433032 | tf_op jit(solution)/shard_map/ppermute | solution.py:54
  69.7 16.6 %collective-permute-start.13 = (bf16[8,64,768]{2,1,0:T(8,128)(2,1)S(1)}, bf16[8,64,768]{2,1,0:T(8,128)(2,1)S(1)}, u32[]{:S(2)}, u32[]{:S(2)}) collective-permute-start(bf16[8,64,768]{2,1,0:T(8,128)(2,1)S(1)} %broadcast_select_fusion.1), channel_id=1, source_target_pairs={{0,8},{8,16},{16,24},{24,0},{1,25},{9,1},{17,9},{25,17},{2,10},{10... | collective-permute-start | bytes 2359304 | tf_op jit(solution)/shard_map/ppermute | solution.py:60
  72.5 22.1 %collective-permute-start.24 = (bf16[4,64,1408]{2,1,0:T(8,128)(2,1)}, bf16[4,64,1408]{2,1,0:T(8,128)(2,1)S(1)}, u32[]{:S(2)}, u32[]{:S(2)}) collective-permute-start(bf16[4,64,1408]{2,1,0:T(8,128)(2,1)} %collective-permute-done.22), channel_id=1, source_target_pairs={{0,32},{32,64},{64,96},{96,128},{128,160},{160,192},{192,224},{224... | collective-permute-start | bytes 2162696 | tf_op jit(solution)/shard_map/ppermute | solution.py:26
  74.1 22.0 %collective-permute-start.25 = (bf16[4,64,1408]{2,1,0:T(8,128)(2,1)S(1)}, bf16[4,64,1408]{2,1,0:T(8,128)(2,1)S(1)}, u32[]{:S(2)}, u32[]{:S(2)}) collective-permute-start(bf16[4,64,1408]{2,1,0:T(8,128)(2,1)S(1)} %collective-permute-done.23), channel_id=1, source_target_pairs={{0,224},{32,0},{64,32},{96,64},{128,96},{160,128},{192,160},{224,1... | collective-permute-start | bytes 2162696 | tf_op jit(solution)/shard_map/ppermute | solution.py:26
  75.5 41.8 %collective-permute-start.31 = (bf16[8,64,704]{2,1,0:T(8,128)(2,1)S(1)}, bf16[8,64,704]{2,1,0:T(8,128)(2,1)S(1)}, u32[]{:S(2)}, u32[]{:S(2)}) collective-permute-start(bf16[8,64,704]{2,1,0:T(8,128)(2,1)S(1)} %broadcast_select_fusion), channel_id=1, source_target_pairs={{0,8},{8,16},{16,24},{24,0},{1,25},{9,1},{17,9},{25,17},{2,10},{10... | collective-permute-start | bytes 2162696 | tf_op jit(solution)/shard_map/ppermute | solution.py:60
  94.6 25.2 %collective-permute-start.26 = (bf16[4,64,1408]{2,1,0:T(8,128)(2,1)S(1)}, bf16[4,64,1408]{2,1,0:T(8,128)(2,1)S(1)}, u32[]{:S(2)}, u32[]{:S(2)}) collective-permute-start(bf16[4,64,1408]{2,1,0:T(8,128)(2,1)S(1)} %collective-permute-done.24), channel_id=1, source_target_pairs={{0,32},{32,64},{64,96},{96,128},{128,160},{160,192},{192,224},{224... | collective-permute-start | bytes 2162696 | tf_op jit(solution)/shard_map/ppermute | solution.py:26
  96.2 23.7 %collective-permute-start.27 = (bf16[4,64,1408]{2,1,0:T(8,128)(2,1)S(1)}, bf16[4,64,1408]{2,1,0:T(8,128)(2,1)S(1)}, u32[]{:S(2)}, u32[]{:S(2)}) collective-permute-start(bf16[4,64,1408]{2,1,0:T(8,128)(2,1)S(1)} %collective-permute-done.25), channel_id=1, source_target_pairs={{0,224},{32,0},{64,32},{96,64},{128,96},{160,128},{192,160},{224,1... | collective-permute-start | bytes 2162696 | tf_op jit(solution)/shard_map/ppermute | solution.py:26
  103.3 8.4 %collective-permute-start.16 = (bf16[128,2048]{1,0:T(8,128)(2,1)S(1)}, bf16[128,2048]{1,0:T(8,128)(2,1)S(1)}, u32[]{:S(2)}, u32[]{:S(2)}) collective-permute-start(bf16[128,2048]{1,0:T(8,128)(2,1)S(1)} %pad_maximum_fusion.2), channel_id=1, source_target_pairs={{0,2},{2,4},{4,6},{6,0},{1,7},{3,1},{5,3},{7,5},{8,10},{10,12},{12... | collective-permute-start | bytes 1572872 | tf_op jit(solution)/shard_map/ppermute | solution.py:60
  111.9 6.9 %collective-permute-start.17 = (bf16[128,2048]{1,0:T(8,128)(2,1)S(1)}, bf16[128,2048]{1,0:T(8,128)(2,1)S(1)}, u32[]{:S(2)}, u32[]{:S(2)}) collective-permute-start(bf16[128,2048]{1,0:T(8,128)(2,1)S(1)} %pad_maximum_fusion.3), channel_id=1, source_target_pairs={{0,1},{1,0},{2,3},{3,2},{4,5},{5,4},{6,7},{7,6},{8,9},{9,8},{10,11... | collective-permute-start | bytes 1572872 | tf_op jit(solution)/shard_map/ppermute | solution.py:54
  119.8 8.4 %collective-permute-start.18 = (bf16[2,64,2048]{2,1,0:T(8,128)(2,1)S(1)}, bf16[2,64,2048]{2,1,0:T(8,128)(2,1)S(1)}, u32[]{:S(2)}, u32[]{:S(2)}) collective-permute-start(bf16[2,64,2048]{2,1,0:T(8,128)(2,1)S(1)} %bitcast.61), channel_id=1, source_target_pairs={{0,2},{2,4},{4,6},{6,0},{1,7},{3,1},{5,3},{7,5},{8,10},{10,12},{12... | collective-permute-start | bytes 1572872 | tf_op jit(solution)/shard_map/ppermute | solution.py:60
  120.0 18.3 %collective-permute-start.28 = (bf16[4,64,1408]{2,1,0:T(8,128)(2,1)S(1)}, bf16[4,64,1408]{2,1,0:T(8,128)(2,1)S(1)}, u32[]{:S(2)}, u32[]{:S(2)}) collective-permute-start(bf16[4,64,1408]{2,1,0:T(8,128)(2,1)S(1)} %broadcast_select_fusion.2), channel_id=1, source_target_pairs={{0,32},{32,64},{64,96},{96,128},{128,160},{160,192},{192,224},{224... | collective-permute-start | bytes 2162696 | tf_op jit(solution)/shard_map/ppermute | solution.py:60
  129.6 8.9 %collective-permute-start.20 = (bf16[2,64,2048]{2,1,0:T(8,128)(2,1)S(1)}, bf16[2,64,2048]{2,1,0:T(8,128)(2,1)S(1)}, u32[]{:S(2)}, u32[]{:S(2)}) collective-permute-start(bf16[2,64,2048]{2,1,0:T(8,128)(2,1)S(1)} %collective-permute-done.18.refs_1_), channel_id=1, source_target_pairs={{0,1},{1,0},{2,3},{3,2},{4,5},{5,4},{6,7},{7,6},{8,9},{9,8},{10,11... | collective-permute-start | bytes 1572872 | tf_op jit(solution)/shard_map/ppermute | solution.py:54
  133.5 6.0 %collective-permute-start.21 = (bf16[64,2048]{1,0:T(8,128)(2,1)S(1)}, bf16[64,2048]{1,0:T(8,128)(2,1)S(1)}, u32[]{:S(2)}, u32[]{:S(2)}) collective-permute-start(bf16[64,2048]{1,0:T(8,128)(2,1)S(1)} %collective-permute-done.19.refs_2_), channel_id=1, source_target_pairs={{0,1},{1,0},{2,3},{3,2},{4,5},{5,4},{6,7},{7,6},{8,9},{9,8},{10,11... | collective-permute-start | bytes 786440 | tf_op jit(solution)/shard_map/ppermute | solution.py:54
  157.3 8.4 %collective-permute-start.34 = (bf16[128,2048]{1,0:T(8,128)(2,1)S(1)}, bf16[128,2048]{1,0:T(8,128)(2,1)S(1)}, u32[]{:S(2)}, u32[]{:S(2)}) collective-permute-start(bf16[128,2048]{1,0:T(8,128)(2,1)S(1)} %pad_maximum_fusion.4), channel_id=1, source_target_pairs={{0,2},{2,4},{4,6},{6,0},{1,7},{3,1},{5,3},{7,5},{8,10},{10,12},{12... | collective-permute-start | bytes 1572872 | tf_op jit(solution)/shard_map/ppermute | solution.py:60
  165.9 5.8 %collective-permute-start.35 = (bf16[64,2048]{1,0:T(8,128)(2,1)S(1)}, bf16[64,2048]{1,0:T(8,128)(2,1)S(1)}, u32[]{:S(2)}, u32[]{:S(2)}) collective-permute-start(bf16[64,2048]{1,0:T(8,128)(2,1)S(1)} %slice.86), channel_id=1, source_target_pairs={{0,1},{1,0},{2,3},{3,2},{4,5},{5,4},{6,7},{7,6},{8,9},{9,8},{10,11... | collective-permute-start | bytes 786440 | tf_op jit(solution)/shard_map/ppermute | solution.py:54
  (11 other events, 209.9 us)

commit v2 on v1

--- a/solution.py
+++ b/solution.py
@@ -165,10 +165,10 @@
 
 
 def mixer_kernel(*refs):
-    x_refs, w_refs = [*refs[0:4], refs[3].at[2]], refs[4:8]
-    taps_ref, recur_ref, inject_ref, slope_ref = refs[8:12]
-    outs, own_ref, gain_ref = refs[12:16], refs[16], refs[17]
-    v_ref, win_ref, wout_ref, gate_ref, in_ref, keep_ref, drive_ref, hid_ref, turned_ref = refs[18:]
+    x_refs, w_refs = refs[0:5], refs[5:9]
+    taps_ref, recur_ref, inject_ref, slope_ref = refs[9:13]
+    outs, own_ref, gain_ref = refs[13:17], refs[17], refs[18]
+    v_ref, win_ref, wout_ref, gate_ref, in_ref, keep_ref, drive_ref, hid_ref, turned_ref = refs[19:]
     mz, mx = lax.axis_index("z"), lax.axis_index("x")
 
     def placed(kz, _):
@@ -245,7 +245,7 @@
     projected(hid_ref, turned_ref, wout_ref, outs)
 
 
-CHUNK = 256
+CHUNK = 128
 TOP = 16
 VMEM = pl.BlockSpec(memory_space=pltpu.VMEM)
 PARTS = tuple(jax.ShapeDtypeStruct((n * OWN, D), bf16) for n in (3, 1, 2, 2))
@@ -356,8 +356,7 @@
     mix_z, down_z = laid(along_z)
     mix_blocks = ring_gathered(mix_z, "x", NX)
     packed = jnp.stack([packed, swapped(packed)])
-    p, far = ring_pieces(packed, "y", NY)
-    x_blocks = [*p, far, swapped(jnp.concatenate([p[1], far[None]], axis=0))]
+    x_blocks = rows_ring(packed)
     up_own = jnp.concatenate([w_up_gate, w_up_value], axis=1)
     sent = jnp.broadcast_to(up_own[None], (NX, *up_own.shape))
     along_x = lax.all_to_all(sent, "x", 0, 0, tiled=True)

time: 182 us -> 188 us (1.033)
  starting transfers between devices: 78.5 us -> 88.3 us
  waiting for transfers between devices: 63.9 us -> 60.1 us
    ppermute x8 -> x9, starting transfers between devices: 34.1 us -> 44.9 us  [swapped(): return lax.ppermute(value, 'c', [(0, 1), (1, 0)])]
    ppermute x12, waiting for transfers between devices: 48.2 us -> 40.5 us  [spread(): return lax.ppermute(value, (axis, 'c'), pairs)]
    ppermute x16, waiting for transfers between devices: 10.2 us -> 14.1 us  [moved(): return lax.ppermute(value, axis, [(i, (i + by) % n) for i in range(n)])]
    ppermute x8 -> x9, waiting for transfers between devices: 5.46 us -> 5.46 us  [swapped(): return lax.ppermute(value, 'c', [(0, 1), (1, 0)])]
  transfers between devices with their start and end apart: 37 -> 38, of which waited for: 16 -> 16; matrix products, arithmetic and copies ran while one was open for 6% -> 5% of each run, Pallas kernels for 4% -> 4%
where the time goes in v2:
time: 188 us
  starting transfers between devices  88.3 us (47%)
  waiting for transfers between devices  60.1 us (32%)
  Pallas kernels  17.4 us (9%)
  blocking collectives  9.25 us (5%)
  other arithmetic  7.14 us (4%)
  local copies, waits for them, and re-layouts  5.04 us (3%)
    ppermute x9, starting transfers between devices, swapped(): return lax.ppermute(value, 'c', [(0, 1), (1, 0)])  44.9 us
    ppermute x12, waiting for transfers between devices, spread(): return lax.ppermute(value, (axis, 'c'), pairs)  40.5 us
    ppermute x16, starting transfers between devices, moved(): return lax.ppermute(value, axis, [(i, (i + by) % n) for i in range(n)])  23.7 us
    ppermute x12, starting transfers between devices, spread(): return lax.ppermute(value, (axis, 'c'), pairs)  15.7 us
    ppermute x16, waiting for transfers between devices, moved(): return lax.ppermute(value, axis, [(i, (i + by) % n) for i in range(n)])  14.1 us
    pallas_call x1, Pallas kernels, ffn(): pl.pallas_call(ffn_kernel, out_shape=PARTS, in_specs=[VMEM] * 8, out_spec...  9.57 us
    all_to_all x1, blocking collectives, shards(): return lax.all_to_all(to_columns, TP, 0, 0, tiled=True).reshape(ROWS, PIECE)  9.25 us
    pallas_call x1, Pallas kernels, mixer(): pl.pallas_call(mixer_kernel, out_shape=(*PARTS, PAIR, jax.ShapeDtypeStruc...  7.73 us
  transfers between devices with their start and end apart: 38, of which 16 were waited for; matrix products, arithmetic and copies ran while one was open for 5% of the time, Pallas kernels for 4%

profile of v2, /device:TPU:1, one launch (start us, length us, event | category | flops | bytes accessed | tf_op | source)
XLA Modules:
  0.0 187.8 jit_solution(8828144970027793380)
XLA Ops:
  0.9 2.5 %collective-permute-start.5 = (bf16[64,1472]{1,0:T(8,128)(2,1)S(1)}, bf16[64,1472]{1,0:T(8,128)(2,1)S(1)}, u32[]{:S(2)}, u32[]{:S(2)}) collective-permute-start(bf16[64,1472]{1,0:T(8,128)(2,1)S(1)} %pad_maximum_fusion.4.refs_0_), channel_id=1, source_target_pairs={{0,32},{32,64},{64,96},{96,128},{128,160},{160,192},{192,224},{224... | collective-permute-start | bytes 565256 | tf_op jit(solution)/shard_map/ppermute | solution.py:26
  3.5 4.0 %collective-permute-start.8 = (bf16[64,1472]{1,0:T(8,128)(2,1)S(1)}, bf16[64,1472]{1,0:T(8,128)(2,1)S(1)}, u32[]{:S(2)}, u32[]{:S(2)}) collective-permute-start(bf16[64,1472]{1,0:T(8,128)(2,1)S(1)} %pad_maximum_fusion.4.refs_0_), channel_id=1, source_target_pairs={{0,224},{32,0},{64,32},{96,64},{128,96},{160,128},{192,160},{224,1... | collective-permute-start | bytes 565256 | tf_op jit(solution)/shard_map/ppermute | solution.py:26
  9.5 4.0 %all-to-all-start = ((bf16[4,64,1408]{2,1,0:T(8,128)(2,1)}), bf16[4,64,1408]{2,1,0:T(8,128)(2,1)S(1)}, u32[]{:S(2)}, u32[]{:S(2)}) async-start(bf16[4,64,1408]{2,1,0:T(8,128)(2,1)} %broadcast_in_dim.56), calls=%async_computation | async-start | bytes 1441792 | tf_op jit(solution)/shard_map/all_to_all | solution.py:362
  16.5 2.7 %collective-permute-start.9 = (bf16[64,1472]{1,0:T(8,128)(2,1)S(1)}, bf16[64,1472]{1,0:T(8,128)(2,1)S(1)}, u32[]{:S(2)}, u32[]{:S(2)}) collective-permute-start(bf16[64,1472]{1,0:T(8,128)(2,1)S(1)} %collective-permute-done.8.refs_7_), channel_id=1, source_target_pairs={{0,224},{32,0},{64,32},{96,64},{128,96},{160,128},{192,160},{224,1... | collective-permute-start | bytes 565256 | tf_op jit(solution)/shard_map/ppermute | solution.py:26
  19.2 4.9 %collective-permute-done.6.refs_2_ = bf16[64,1472]{1,0:T(8,128)(2,1)S(1)} collective-permute-done((bf16[64,1472]{1,0:T(8,128)(2,1)S(1)}, bf16[64,1472]{1,0:T(8,128)(2,1)S(1)}, u32[]{:S(2)}, u32[]{:S(2)}) %collective-permute-start.6) | collective-permute-done | bytes 188448 | tf_op jit(solution)/shard_map/ppermute | solution.py:26
  24.1 2.7 %collective-permute-start.10 = (bf16[64,1472]{1,0:T(8,128)(2,1)S(1)}, bf16[64,1472]{1,0:T(8,128)(2,1)S(1)}, u32[]{:S(2)}, u32[]{:S(2)}) collective-permute-start(bf16[64,1472]{1,0:T(8,128)(2,1)S(1)} %collective-permute-done.9.refs_6_), channel_id=1, source_target_pairs={{0,224},{32,0},{64,32},{96,64},{128,96},{160,128},{192,160},{224,1... | collective-permute-start | bytes 565256 | tf_op jit(solution)/shard_map/ppermute | solution.py:26
  26.8 2.8 %collective-permute-start.1 = (bf16[2,528,256]{2,1,0:T(8,128)(2,1)S(1)}, bf16[2,528,256]{2,1,0:T(8,128)(2,1)S(1)}, u32[]{:S(2)}, u32[]{:S(2)}) collective-permute-start(bf16[2,528,256]{2,1,0:T(8,128)(2,1)S(1)} %pad_maximum_fusion.refs_0_), channel_id=1, source_target_pairs={{0,2},{2,4},{4,6},{6,0},{1,7},{3,1},{5,3},{7,5},{8,10},{10,12},{12... | collective-permute-start | bytes 1622024 | tf_op jit(solution)/shard_map/ppermute | solution.py:60
  31.5 2.4 %collective-permute-start.11 = (bf16[64,1472]{1,0:T(8,128)(2,1)}, bf16[64,1472]{1,0:T(8,128)(2,1)S(1)}, u32[]{:S(2)}, u32[]{:S(2)}) collective-permute-start(bf16[64,1472]{1,0:T(8,128)(2,1)} %broadcast_select_fusion.3), channel_id=1, source_target_pairs={{0,32},{32,64},{64,96},{96,128},{128,160},{160,192},{192,224},{224... | collective-permute-start | bytes 565256 | tf_op jit(solution)/shard_map/ppermute | solution.py:60
  33.9 2.9 %collective-permute-done.11.refs_4_ = bf16[64,1472]{1,0:T(8,128)(2,1)S(1)} collective-permute-done((bf16[64,1472]{1,0:T(8,128)(2,1)}, bf16[64,1472]{1,0:T(8,128)(2,1)S(1)}, u32[]{:S(2)}, u32[]{:S(2)}) %collective-permute-start.11) | collective-permute-done | bytes 188448 | tf_op jit(solution)/shard_map/ppermute | solution.py:60
  37.0 1.8 collective-permute-start.12
  40.3 8.0 %collective-permute-done.23 = bf16[4,64,1408]{2,1,0:T(8,128)(2,1)} collective-permute-done((bf16[4,64,1408]{2,1,0:T(8,128)(2,1)S(1)}, bf16[4,64,1408]{2,1,0:T(8,128)(2,1)}, u32[]{:S(2)}, u32[]{:S(2)}) %collective-permute-start.23) | collective-permute-done | bytes 720928 | tf_op jit(solution)/shard_map/ppermute | solution.py:26
  48.3 3.0 %collective-permute-start.31 = (bf16[8,64,704]{2,1,0:T(8,128)(2,1)S(1)}, bf16[8,64,704]{2,1,0:T(8,128)(2,1)S(1)}, u32[]{:S(2)}, u32[]{:S(2)}) collective-permute-start(bf16[8,64,704]{2,1,0:T(8,128)(2,1)S(1)} %get-tuple-element.32), channel_id=1, source_target_pairs={{0,24},{8,0},{16,8},{24,16},{1,25},{9,1},{17,9},{25,17},{2,26},{10... | collective-permute-start | bytes 2162696 | tf_op jit(solution)/shard_map/ppermute | solution.py:26
  55.5 3.5 %collective-permute-done.2.refs_2_ = bf16[528,256]{1,0:T(8,128)(2,1)S(1)} collective-permute-done((bf16[528,256]{1,0:T(8,128)(2,1)S(1)}, bf16[528,256]{1,0:T(8,128)(2,1)S(1)}, u32[]{:S(2)}, u32[]{:S(2)}) %collective-permute-start.2) | collective-permute-done | bytes 270368 | tf_op jit(solution)/shard_map/ppermute | solution.py:60
  58.9 17.0 %collective-permute-start.3 = (bf16[2,528,256]{2,1,0:T(8,128)(2,1)S(1)}, bf16[2,528,256]{2,1,0:T(8,128)(2,1)S(1)}, u32[]{:S(2)}, u32[]{:S(2)}) collective-permute-start(bf16[2,528,256]{2,1,0:T(8,128)(2,1)S(1)} %collective-permute-done.1.refs_1_), channel_id=1, source_target_pairs={{0,1},{1,0},{2,3},{3,2},{4,5},{5,4},{6,7},{7,6},{8,9},{9,8},{10,11... | collective-permute-start | bytes 1622024 | tf_op jit(solution)/shard_map/ppermute | solution.py:54
  76.3 2.7 %collective-permute-start.26 = (bf16[4,64,1408]{2,1,0:T(8,128)(2,1)S(1)}, bf16[4,64,1408]{2,1,0:T(8,128)(2,1)S(1)}, u32[]{:S(2)}, u32[]{:S(2)}) collective-permute-start(bf16[4,64,1408]{2,1,0:T(8,128)(2,1)S(1)} %collective-permute-done.24), channel_id=1, source_target_pairs={{0,224},{32,0},{64,32},{96,64},{128,96},{160,128},{192,160},{224,1... | collective-permute-start | bytes 2162696 | tf_op jit(solution)/shard_map/ppermute | solution.py:26
  79.0 1.6 collective-permute-start.32
  81.5 7.7 %mixer.1 = (bf16[192,2048]{1,0:T(8,128)(2,1)S(1)}, bf16[64,2048]{1,0:T(8,128)(2,1)S(1)}, bf16[128,2048]{1,0:T(8,128)(2,1)S(1)}, bf16[128,2048]{1,0:T(8,128)(2,1)...) custom-call(bf16[2,528,256]{2,1,0:T(8,128)(2,1)S(1)} %pad_maximum_fusion.refs_0_, ...), custom_call_target="tpu_custom_call" | custom-call | flops 1744830464 | bytes 8388608 | tf_op jit(solution)/shard_map/mixer/pallas_call | solution.py:256
  89.2 10.9 %collective-permute-start.15 = (bf16[192,2048]{1,0:T(8,128)(2,1)S(1)}, bf16[192,2048]{1,0:T(8,128)(2,1)S(1)}, u32[]{:S(2)}, u32[]{:S(2)}) collective-permute-start(bf16[192,2048]{1,0:T(8,128)(2,1)S(1)} %get-tuple-element.28), channel_id=1, source_target_pairs={{0,1},{1,0},{2,3},{3,2},{4,5},{5,4},{6,7},{7,6},{8,9},{9,8},{10,11... | collective-permute-start | bytes 2359304 | tf_op jit(solution)/shard_map/ppermute | solution.py:54
  101.3 2.2 %collective-permute-start.28 = (bf16[4,64,1408]{2,1,0:T(8,128)(2,1)S(1)}, bf16[4,64,1408]{2,1,0:T(8,128)(2,1)S(1)}, u32[]{:S(2)}, u32[]{:S(2)}) collective-permute-start(bf16[4,64,1408]{2,1,0:T(8,128)(2,1)S(1)} %collective-permute-done.26), channel_id=1, source_target_pairs={{0,224},{32,0},{64,32},{96,64},{128,96},{160,128},{192,160},{224,1... | collective-permute-start | bytes 2162696 | tf_op jit(solution)/shard_map/ppermute | solution.py:26
  105.4 4.0 %collective-permute-done.16 = bf16[64,2048]{1,0:T(8,128)(2,1)S(1)} collective-permute-done((bf16[64,2048]{1,0:T(8,128)(2,1)S(1)}, bf16[64,2048]{1,0:T(8,128)(2,1)S(1)}, u32[]{:S(2)}, u32[]{:S(2)}) %collective-permute-start.16) | collective-permute-done | bytes 262176 | tf_op jit(solution)/shard_map/ppermute | solution.py:60
  109.4 2.9 %collective-permute-start.17 = (bf16[128,2048]{1,0:T(8,128)(2,1)S(1)}, bf16[128,2048]{1,0:T(8,128)(2,1)S(1)}, u32[]{:S(2)}, u32[]{:S(2)}) collective-permute-start(bf16[128,2048]{1,0:T(8,128)(2,1)S(1)} %pad_maximum_fusion.1), channel_id=1, source_target_pairs={{0,2},{2,4},{4,6},{6,0},{1,7},{3,1},{5,3},{7,5},{8,10},{10,12},{12... | collective-permute-start | bytes 1572872 | tf_op jit(solution)/shard_map/ppermute | solution.py:60
  112.5 5.9 %collective-permute-done.17 = bf16[128,2048]{1,0:T(8,128)(2,1)S(1)} collective-permute-done((bf16[128,2048]{1,0:T(8,128)(2,1)S(1)}, bf16[128,2048]{1,0:T(8,128)(2,1)S(1)}, u32[]{:S(2)}, u32[]{:S(2)}) %collective-permute-start.17) | collective-permute-done | bytes 524320 | tf_op jit(solution)/shard_map/ppermute | solution.py:60
  118.7 4.4 %collective-permute-start.18 = (bf16[128,2048]{1,0:T(8,128)(2,1)S(1)}, bf16[128,2048]{1,0:T(8,128)(2,1)S(1)}, u32[]{:S(2)}, u32[]{:S(2)}) collective-permute-start(bf16[128,2048]{1,0:T(8,128)(2,1)S(1)} %pad_maximum_fusion.2), channel_id=1, source_target_pairs={{0,1},{1,0},{2,3},{3,2},{4,5},{5,4},{6,7},{7,6},{8,9},{9,8},{10,11... | collective-permute-start | bytes 1572872 | tf_op jit(solution)/shard_map/ppermute | solution.py:54
  125.9 8.0 %collective-permute-done.19.refs_1_ = bf16[2,64,2048]{2,1,0:T(8,128)(2,1)S(1)} collective-permute-done((bf16[2,64,2048]{2,1,0:T(8,128)(2,1)S(1)}, bf16[2,64,2048]{2,1,0:T(8,128)(2,1)S(1)}, u32[]{:S(2)}, u32[]{:S(2)}) %collective-permute-start.19) | collective-permute-done | bytes 524320 | tf_op jit(solution)/shard_map/ppermute | solution.py:60
  136.7 2.6 %collective-permute-done.20.refs_2_ = bf16[64,2048]{1,0:T(8,128)(2,1)S(1)} collective-permute-done((bf16[64,2048]{1,0:T(8,128)(2,1)S(1)}, bf16[64,2048]{1,0:T(8,128)(2,1)S(1)}, u32[]{:S(2)}, u32[]{:S(2)}) %collective-permute-start.20) | collective-permute-done | bytes 262176 | tf_op jit(solution)/shard_map/ppermute | solution.py:60
  139.3 4.8 %collective-permute-start.22 = (bf16[64,2048]{1,0:T(8,128)(2,1)S(1)}, bf16[64,2048]{1,0:T(8,128)(2,1)S(1)}, u32[]{:S(2)}, u32[]{:S(2)}) collective-permute-start(bf16[64,2048]{1,0:T(8,128)(2,1)S(1)} %collective-permute-done.20.refs_2_), channel_id=1, source_target_pairs={{0,1},{1,0},{2,3},{3,2},{4,5},{5,4},{6,7},{7,6},{8,9},{9,8},{10,11... | collective-permute-start | bytes 786440 | tf_op jit(solution)/shard_map/ppermute | solution.py:54
  145.2 9.6 %ffn.1 = (bf16[192,2048]{1,0:T(8,128)(2,1)S(1)}, bf16[64,2048]{1,0:T(8,128)(2,1)S(1)}, bf16[128,2048]{1,0:T(8,128)(2,1)S(1)}, bf16[128,2048]{1,0:T(8,128)(2,1)S(1)}) custom-call(bf16[2,64,2048]{2,1,0:T(8,128)(2,1)S(1)} %bitcast.61, bf16[2,64,2048]{2,1,0:T(8,128)(2,1)S(1)} %collective-permute-done.19.refs_1_, ...), custom_call_target="tpu_custom_call" | custom-call | flops 4429185024 | bytes 13631488 | tf_op jit(solution)/shard_map/ffn/pallas_call | solution.py:326
  155.3 1.9 %collective-permute-done.33 = bf16[192,2048]{1,0:T(8,128)(2,1)S(1)} collective-permute-done((bf16[192,2048]{1,0:T(8,128)(2,1)S(1)}, bf16[192,2048]{1,0:T(8,128)(2,1)S(1)}, u32[]{:S(2)}, u32[]{:S(2)}) %collective-permute-start.33) | collective-permute-done | bytes 786464 | tf_op jit(solution)/shard_map/ppermute | solution.py:54
  157.7 5.3 %collective-permute-done.34 = bf16[64,2048]{1,0:T(8,128)(2,1)S(1)} collective-permute-done((bf16[64,2048]{1,0:T(8,128)(2,1)S(1)}, bf16[64,2048]{1,0:T(8,128)(2,1)S(1)}, u32[]{:S(2)}, u32[]{:S(2)}) %collective-permute-start.34) | collective-permute-done | bytes 262176 | tf_op jit(solution)/shard_map/ppermute | solution.py:60
  164.1 7.4 %collective-permute-done.35 = bf16[128,2048]{1,0:T(8,128)(2,1)S(1)} collective-permute-done((bf16[128,2048]{1,0:T(8,128)(2,1)S(1)}, bf16[128,2048]{1,0:T(8,128)(2,1)S(1)}, u32[]{:S(2)}, u32[]{:S(2)}) %collective-permute-start.35) | collective-permute-done | bytes 524320 | tf_op jit(solution)/shard_map/ppermute | solution.py:60
  171.7 4.6 %collective-permute-start.36 = (bf16[64,2048]{1,0:T(8,128)(2,1)S(1)}, bf16[64,2048]{1,0:T(8,128)(2,1)S(1)}, u32[]{:S(2)}, u32[]{:S(2)}) collective-permute-start(bf16[64,2048]{1,0:T(8,128)(2,1)S(1)} %slice.86), channel_id=1, source_target_pairs={{0,1},{1,0},{2,3},{3,2},{4,5},{5,4},{6,7},{7,6},{8,9},{9,8},{10,11... | collective-permute-start | bytes 786440 | tf_op jit(solution)/shard_map/ppermute | solution.py:54
  177.8 9.2 %all_to_all.10 = bf16[8,64,256]{2,1,0:T(8,128)(2,1)S(1)} all-to-all(bf16[8,64,256]{2,1,0:T(8,128)(2,1)S(1)} %bitcast.65), channel_id=1, replica_groups=mesh['z'=8,'x'=4,'y'=4,'c'=2] {'y','c'}, dimensions={0} | all-to-all | bytes 524288 | tf_op jit(solution)/shard_map/all_to_all | solution.py:382
  (117 shorter events, 29.3 us)
Async XLA Ops:
  0.9 15.6 %collective-permute-start.5 = (bf16[64,1472]{1,0:T(8,128)(2,1)S(1)}, bf16[64,1472]{1,0:T(8,128)(2,1)S(1)}, u32[]{:S(2)}, u32[]{:S(2)}) collective-permute-start(bf16[64,1472]{1,0:T(8,128)(2,1)S(1)} %pad_maximum_fusion.4.refs_0_), channel_id=1, source_target_pairs={{0,32},{32,64},{64,96},{96,128},{128,160},{160,192},{192,224},{224... | collective-permute-start | bytes 565256 | tf_op jit(solution)/shard_map/ppermute | solution.py:26
  3.5 13.0 %collective-permute-start.8 = (bf16[64,1472]{1,0:T(8,128)(2,1)S(1)}, bf16[64,1472]{1,0:T(8,128)(2,1)S(1)}, u32[]{:S(2)}, u32[]{:S(2)}) collective-permute-start(bf16[64,1472]{1,0:T(8,128)(2,1)S(1)} %pad_maximum_fusion.4.refs_0_), channel_id=1, source_target_pairs={{0,224},{32,0},{64,32},{96,64},{128,96},{160,128},{192,160},{224,1... | collective-permute-start | bytes 565256 | tf_op jit(solution)/shard_map/ppermute | solution.py:26
  9.5 20.2 %all-to-all-start = ((bf16[4,64,1408]{2,1,0:T(8,128)(2,1)}), bf16[4,64,1408]{2,1,0:T(8,128)(2,1)S(1)}, u32[]{:S(2)}, u32[]{:S(2)}) async-start(bf16[4,64,1408]{2,1,0:T(8,128)(2,1)} %broadcast_in_dim.56), calls=%async_computation | async-start | bytes 1441792 | tf_op jit(solution)/shard_map/all_to_all | solution.py:362
  15.2 11.6 %collective-permute-start = (bf16[528,256]{1,0:T(8,128)(2,1)S(1)}, bf16[528,256]{1,0:T(8,128)(2,1)S(1)}, u32[]{:S(2)}, u32[]{:S(2)}) collective-permute-start(bf16[528,256]{1,0:T(8,128)(2,1)S(1)} %get-tuple-element.44), channel_id=1, source_target_pairs={{0,1},{1,0},{2,3},{3,2},{4,5},{5,4},{6,7},{7,6},{8,9},{9,8},{10,11... | collective-permute-start | bytes 811016 | tf_op jit(solution)/shard_map/ppermute | solution.py:54
  16.5 7.6 %collective-permute-start.6 = (bf16[64,1472]{1,0:T(8,128)(2,1)S(1)}, bf16[64,1472]{1,0:T(8,128)(2,1)S(1)}, u32[]{:S(2)}, u32[]{:S(2)}) collective-permute-start(bf16[64,1472]{1,0:T(8,128)(2,1)S(1)} %collective-permute-done.5.refs_1_), channel_id=1, source_target_pairs={{0,32},{32,64},{64,96},{96,128},{128,160},{160,192},{192,224},{224... | collective-permute-start | bytes 565256 | tf_op jit(solution)/shard_map/ppermute | solution.py:26
  16.5 7.6 %collective-permute-start.9 = (bf16[64,1472]{1,0:T(8,128)(2,1)S(1)}, bf16[64,1472]{1,0:T(8,128)(2,1)S(1)}, u32[]{:S(2)}, u32[]{:S(2)}) collective-permute-start(bf16[64,1472]{1,0:T(8,128)(2,1)S(1)} %collective-permute-done.8.refs_7_), channel_id=1, source_target_pairs={{0,224},{32,0},{64,32},{96,64},{128,96},{160,128},{192,160},{224,1... | collective-permute-start | bytes 565256 | tf_op jit(solution)/shard_map/ppermute | solution.py:26
  24.1 6.7 %collective-permute-start.7 = (bf16[64,1472]{1,0:T(8,128)(2,1)S(1)}, bf16[64,1472]{1,0:T(8,128)(2,1)S(1)}, u32[]{:S(2)}, u32[]{:S(2)}) collective-permute-start(bf16[64,1472]{1,0:T(8,128)(2,1)S(1)} %collective-permute-done.6.refs_2_), channel_id=1, source_target_pairs={{0,32},{32,64},{64,96},{96,128},{128,160},{160,192},{192,224},{224... | collective-permute-start | bytes 565256 | tf_op jit(solution)/shard_map/ppermute | solution.py:26
  24.1 6.7 %collective-permute-start.10 = (bf16[64,1472]{1,0:T(8,128)(2,1)S(1)}, bf16[64,1472]{1,0:T(8,128)(2,1)S(1)}, u32[]{:S(2)}, u32[]{:S(2)}) collective-permute-start(bf16[64,1472]{1,0:T(8,128)(2,1)S(1)} %collective-permute-done.9.refs_6_), channel_id=1, source_target_pairs={{0,224},{32,0},{64,32},{96,64},{128,96},{160,128},{192,160},{224,1... | collective-permute-start | bytes 565256 | tf_op jit(solution)/shard_map/ppermute | solution.py:26
  26.8 13.3 %collective-permute-start.1 = (bf16[2,528,256]{2,1,0:T(8,128)(2,1)S(1)}, bf16[2,528,256]{2,1,0:T(8,128)(2,1)S(1)}, u32[]{:S(2)}, u32[]{:S(2)}) collective-permute-start(bf16[2,528,256]{2,1,0:T(8,128)(2,1)S(1)} %pad_maximum_fusion.refs_0_), channel_id=1, source_target_pairs={{0,2},{2,4},{4,6},{6,0},{1,7},{3,1},{5,3},{7,5},{8,10},{10,12},{12... | collective-permute-start | bytes 1622024 | tf_op jit(solution)/shard_map/ppermute | solution.py:60
  29.6 18.7 %collective-permute-start.23 = (bf16[4,64,1408]{2,1,0:T(8,128)(2,1)S(1)}, bf16[4,64,1408]{2,1,0:T(8,128)(2,1)}, u32[]{:S(2)}, u32[]{:S(2)}) collective-permute-start(bf16[4,64,1408]{2,1,0:T(8,128)(2,1)S(1)} %all-to-all-done), channel_id=1, source_target_pairs={{0,32},{32,64},{64,96},{96,128},{128,160},{160,192},{192,224},{224... | collective-permute-start | bytes 2162696 | tf_op jit(solution)/shard_map/ppermute | solution.py:26
  33.9 42.1 %collective-permute-start.24 = (bf16[4,64,1408]{2,1,0:T(8,128)(2,1)S(1)}, bf16[4,64,1408]{2,1,0:T(8,128)(2,1)S(1)}, u32[]{:S(2)}, u32[]{:S(2)}) collective-permute-start(bf16[4,64,1408]{2,1,0:T(8,128)(2,1)S(1)} %all-to-all-done), channel_id=1, source_target_pairs={{0,224},{32,0},{64,32},{96,64},{128,96},{160,128},{192,160},{224,1... | collective-permute-start | bytes 2162696 | tf_op jit(solution)/shard_map/ppermute | solution.py:26
  37.0 16.3 %collective-permute-start.12 = (bf16[8,64,768]{2,1,0:T(8,128)(2,1)S(1)}, bf16[8,64,768]{2,1,0:T(8,128)(2,1)S(1)}, u32[]{:S(2)}, u32[]{:S(2)}) collective-permute-start(bf16[8,64,768]{2,1,0:T(8,128)(2,1)S(1)} %get-tuple-element.23.refs_5_), channel_id=1, source_target_pairs={{0,8},{8,16},{16,24},{24,0},{1,9},{9,17},{17,25},{25,1},{2,10},{10... | collective-permute-start | bytes 2359304 | tf_op jit(solution)/shard_map/ppermute | solution.py:26
  38.8 15.8 %collective-permute-start.13 = (bf16[8,64,768]{2,1,0:T(8,128)(2,1)S(1)}, bf16[8,64,768]{2,1,0:T(8,128)(2,1)S(1)}, u32[]{:S(2)}, u32[]{:S(2)}) collective-permute-start(bf16[8,64,768]{2,1,0:T(8,128)(2,1)S(1)} %get-tuple-element.23.refs_5_), channel_id=1, source_target_pairs={{0,24},{8,0},{16,8},{24,16},{1,25},{9,1},{17,9},{25,17},{2,26},{10... | collective-permute-start | bytes 2359304 | tf_op jit(solution)/shard_map/ppermute | solution.py:26
  40.1 36.1 %collective-permute-start.30 = (bf16[8,64,704]{2,1,0:T(8,128)(2,1)S(1)}, bf16[8,64,704]{2,1,0:T(8,128)(2,1)S(1)}, u32[]{:S(2)}, u32[]{:S(2)}) collective-permute-start(bf16[8,64,704]{2,1,0:T(8,128)(2,1)S(1)} %get-tuple-element.32), channel_id=1, source_target_pairs={{0,8},{8,16},{16,24},{24,0},{1,9},{9,17},{17,25},{25,1},{2,10},{10... | collective-permute-start | bytes 2162696 | tf_op jit(solution)/shard_map/ppermute | solution.py:26
  48.3 28.0 %collective-permute-start.31 = (bf16[8,64,704]{2,1,0:T(8,128)(2,1)S(1)}, bf16[8,64,704]{2,1,0:T(8,128)(2,1)S(1)}, u32[]{:S(2)}, u32[]{:S(2)}) collective-permute-start(bf16[8,64,704]{2,1,0:T(8,128)(2,1)S(1)} %get-tuple-element.32), channel_id=1, source_target_pairs={{0,24},{8,0},{16,8},{24,16},{1,25},{9,1},{17,9},{25,17},{2,26},{10... | collective-permute-start | bytes 2162696 | tf_op jit(solution)/shard_map/ppermute | solution.py:26
  53.3 5.7 %collective-permute-start.2 = (bf16[528,256]{1,0:T(8,128)(2,1)S(1)}, bf16[528,256]{1,0:T(8,128)(2,1)S(1)}, u32[]{:S(2)}, u32[]{:S(2)}) collective-permute-start(bf16[528,256]{1,0:T(8,128)(2,1)S(1)} %slice_bitcast_fusion), channel_id=1, source_target_pairs={{0,2},{2,4},{4,6},{6,0},{1,7},{3,1},{5,3},{7,5},{8,10},{10,12},{12... | collective-permute-start | bytes 811016 | tf_op jit(solution)/shard_map/ppermute | solution.py:60
  54.7 26.8 %collective-permute-start.14 = (bf16[8,64,768]{2,1,0:T(8,128)(2,1)S(1)}, bf16[8,64,768]{2,1,0:T(8,128)(2,1)S(1)}, u32[]{:S(2)}, u32[]{:S(2)}) collective-permute-start(bf16[8,64,768]{2,1,0:T(8,128)(2,1)S(1)} %broadcast_select_fusion.1), channel_id=1, source_target_pairs={{0,8},{8,16},{16,24},{24,0},{1,25},{9,1},{17,9},{25,17},{2,10},{10... | collective-permute-start | bytes 2359304 | tf_op jit(solution)/shard_map/ppermute | solution.py:60
  58.9 20.1 %collective-permute-start.3 = (bf16[2,528,256]{2,1,0:T(8,128)(2,1)S(1)}, bf16[2,528,256]{2,1,0:T(8,128)(2,1)S(1)}, u32[]{:S(2)}, u32[]{:S(2)}) collective-permute-start(bf16[2,528,256]{2,1,0:T(8,128)(2,1)S(1)} %collective-permute-done.1.refs_1_), channel_id=1, source_target_pairs={{0,1},{1,0},{2,3},{3,2},{4,5},{5,4},{6,7},{7,6},{8,9},{9,8},{10,11... | collective-permute-start | bytes 1622024 | tf_op jit(solution)/shard_map/ppermute | solution.py:54
  76.2 24.6 %collective-permute-start.25 = (bf16[4,64,1408]{2,1,0:T(8,128)(2,1)}, bf16[4,64,1408]{2,1,0:T(8,128)(2,1)S(1)}, u32[]{:S(2)}, u32[]{:S(2)}) collective-permute-start(bf16[4,64,1408]{2,1,0:T(8,128)(2,1)} %collective-permute-done.23), channel_id=1, source_target_pairs={{0,32},{32,64},{64,96},{96,128},{128,160},{160,192},{192,224},{224... | collective-permute-start | bytes 2162696 | tf_op jit(solution)/shard_map/ppermute | solution.py:26
  76.3 25.0 %collective-permute-start.26 = (bf16[4,64,1408]{2,1,0:T(8,128)(2,1)S(1)}, bf16[4,64,1408]{2,1,0:T(8,128)(2,1)S(1)}, u32[]{:S(2)}, u32[]{:S(2)}) collective-permute-start(bf16[4,64,1408]{2,1,0:T(8,128)(2,1)S(1)} %collective-permute-done.24), channel_id=1, source_target_pairs={{0,224},{32,0},{64,32},{96,64},{128,96},{160,128},{192,160},{224,1... | collective-permute-start | bytes 2162696 | tf_op jit(solution)/shard_map/ppermute | solution.py:26
  79.0 44.1 %collective-permute-start.32 = (bf16[8,64,704]{2,1,0:T(8,128)(2,1)S(1)}, bf16[8,64,704]{2,1,0:T(8,128)(2,1)S(1)}, u32[]{:S(2)}, u32[]{:S(2)}) collective-permute-start(bf16[8,64,704]{2,1,0:T(8,128)(2,1)S(1)} %broadcast_select_fusion), channel_id=1, source_target_pairs={{0,8},{8,16},{16,24},{24,0},{1,25},{9,1},{17,9},{25,17},{2,10},{10... | collective-permute-start | bytes 2162696 | tf_op jit(solution)/shard_map/ppermute | solution.py:60
  89.2 14.3 %collective-permute-start.15 = (bf16[192,2048]{1,0:T(8,128)(2,1)S(1)}, bf16[192,2048]{1,0:T(8,128)(2,1)S(1)}, u32[]{:S(2)}, u32[]{:S(2)}) collective-permute-start(bf16[192,2048]{1,0:T(8,128)(2,1)S(1)} %get-tuple-element.28), channel_id=1, source_target_pairs={{0,1},{1,0},{2,3},{3,2},{4,5},{5,4},{6,7},{7,6},{8,9},{9,8},{10,11... | collective-permute-start | bytes 2359304 | tf_op jit(solution)/shard_map/ppermute | solution.py:54
  100.7 24.9 %collective-permute-start.27 = (bf16[4,64,1408]{2,1,0:T(8,128)(2,1)S(1)}, bf16[4,64,1408]{2,1,0:T(8,128)(2,1)S(1)}, u32[]{:S(2)}, u32[]{:S(2)}) collective-permute-start(bf16[4,64,1408]{2,1,0:T(8,128)(2,1)S(1)} %collective-permute-done.25), channel_id=1, source_target_pairs={{0,32},{32,64},{64,96},{96,128},{128,160},{160,192},{192,224},{224... | collective-permute-start | bytes 2162696 | tf_op jit(solution)/shard_map/ppermute | solution.py:26
  101.3 24.3 %collective-permute-start.28 = (bf16[4,64,1408]{2,1,0:T(8,128)(2,1)S(1)}, bf16[4,64,1408]{2,1,0:T(8,128)(2,1)S(1)}, u32[]{:S(2)}, u32[]{:S(2)}) collective-permute-start(bf16[4,64,1408]{2,1,0:T(8,128)(2,1)S(1)} %collective-permute-done.26), channel_id=1, source_target_pairs={{0,224},{32,0},{64,32},{96,64},{128,96},{160,128},{192,160},{224,1... | collective-permute-start | bytes 2162696 | tf_op jit(solution)/shard_map/ppermute | solution.py:26
  109.4 9.0 %collective-permute-start.17 = (bf16[128,2048]{1,0:T(8,128)(2,1)S(1)}, bf16[128,2048]{1,0:T(8,128)(2,1)S(1)}, u32[]{:S(2)}, u32[]{:S(2)}) collective-permute-start(bf16[128,2048]{1,0:T(8,128)(2,1)S(1)} %pad_maximum_fusion.1), channel_id=1, source_target_pairs={{0,2},{2,4},{4,6},{6,0},{1,7},{3,1},{5,3},{7,5},{8,10},{10,12},{12... | collective-permute-start | bytes 1572872 | tf_op jit(solution)/shard_map/ppermute | solution.py:60
  118.7 5.9 %collective-permute-start.18 = (bf16[128,2048]{1,0:T(8,128)(2,1)S(1)}, bf16[128,2048]{1,0:T(8,128)(2,1)S(1)}, u32[]{:S(2)}, u32[]{:S(2)}) collective-permute-start(bf16[128,2048]{1,0:T(8,128)(2,1)S(1)} %pad_maximum_fusion.2), channel_id=1, source_target_pairs={{0,1},{1,0},{2,3},{3,2},{4,5},{5,4},{6,7},{7,6},{8,9},{9,8},{10,11... | collective-permute-start | bytes 1572872 | tf_op jit(solution)/shard_map/ppermute | solution.py:54
  125.6 8.4 %collective-permute-start.19 = (bf16[2,64,2048]{2,1,0:T(8,128)(2,1)S(1)}, bf16[2,64,2048]{2,1,0:T(8,128)(2,1)S(1)}, u32[]{:S(2)}, u32[]{:S(2)}) collective-permute-start(bf16[2,64,2048]{2,1,0:T(8,128)(2,1)S(1)} %bitcast.60), channel_id=1, source_target_pairs={{0,2},{2,4},{4,6},{6,0},{1,7},{3,1},{5,3},{7,5},{8,10},{10,12},{12... | collective-permute-start | bytes 1572872 | tf_op jit(solution)/shard_map/ppermute | solution.py:60
  125.8 18.3 %collective-permute-start.29 = (bf16[4,64,1408]{2,1,0:T(8,128)(2,1)S(1)}, bf16[4,64,1408]{2,1,0:T(8,128)(2,1)S(1)}, u32[]{:S(2)}, u32[]{:S(2)}) collective-permute-start(bf16[4,64,1408]{2,1,0:T(8,128)(2,1)S(1)} %broadcast_select_fusion.2), channel_id=1, source_target_pairs={{0,32},{32,64},{64,96},{96,128},{128,160},{160,192},{192,224},{224... | collective-permute-start | bytes 2162696 | tf_op jit(solution)/shard_map/ppermute | solution.py:60
  135.4 8.9 %collective-permute-start.21 = (bf16[2,64,2048]{2,1,0:T(8,128)(2,1)S(1)}, bf16[2,64,2048]{2,1,0:T(8,128)(2,1)S(1)}, u32[]{:S(2)}, u32[]{:S(2)}) collective-permute-start(bf16[2,64,2048]{2,1,0:T(8,128)(2,1)S(1)} %collective-permute-done.19.refs_1_), channel_id=1, source_target_pairs={{0,1},{1,0},{2,3},{3,2},{4,5},{5,4},{6,7},{7,6},{8,9},{9,8},{10,11... | collective-permute-start | bytes 1572872 | tf_op jit(solution)/shard_map/ppermute | solution.py:54
  139.3 6.0 %collective-permute-start.22 = (bf16[64,2048]{1,0:T(8,128)(2,1)S(1)}, bf16[64,2048]{1,0:T(8,128)(2,1)S(1)}, u32[]{:S(2)}, u32[]{:S(2)}) collective-permute-start(bf16[64,2048]{1,0:T(8,128)(2,1)S(1)} %collective-permute-done.20.refs_2_), channel_id=1, source_target_pairs={{0,1},{1,0},{2,3},{3,2},{4,5},{5,4},{6,7},{7,6},{8,9},{9,8},{10,11... | collective-permute-start | bytes 786440 | tf_op jit(solution)/shard_map/ppermute | solution.py:54
  163.1 8.4 %collective-permute-start.35 = (bf16[128,2048]{1,0:T(8,128)(2,1)S(1)}, bf16[128,2048]{1,0:T(8,128)(2,1)S(1)}, u32[]{:S(2)}, u32[]{:S(2)}) collective-permute-start(bf16[128,2048]{1,0:T(8,128)(2,1)S(1)} %pad_maximum_fusion.3), channel_id=1, source_target_pairs={{0,2},{2,4},{4,6},{6,0},{1,7},{3,1},{5,3},{7,5},{8,10},{10,12},{12... | collective-permute-start | bytes 1572872 | tf_op jit(solution)/shard_map/ppermute | solution.py:60
  171.7 5.8 %collective-permute-start.36 = (bf16[64,2048]{1,0:T(8,128)(2,1)S(1)}, bf16[64,2048]{1,0:T(8,128)(2,1)S(1)}, u32[]{:S(2)}, u32[]{:S(2)}) collective-permute-start(bf16[64,2048]{1,0:T(8,128)(2,1)S(1)} %slice.86), channel_id=1, source_target_pairs={{0,1},{1,0},{2,3},{3,2},{4,5},{5,4},{6,7},{7,6},{8,9},{9,8},{10,11... | collective-permute-start | bytes 786440 | tf_op jit(solution)/shard_map/ppermute | solution.py:54
  (12 other events, 199.7 us)

commit v3 on v2

--- a/solution.py
+++ b/solution.py
@@ -192,8 +192,8 @@
         gain_ref[:, at] = ref[ROWS : ROWS + 8, :]
 
     def normed(i, _):
-        rows = stretch(i, 128)
-        squares = jnp.zeros((128, 1), f32)
+        rows = stretch(i, 64)
+        squares = jnp.zeros((64, 1), f32)
         for ref, _at in xs:
             v = ref[rows, :].astype(f32)
             squares = squares + jnp.sum(v * v, axis=1, keepdims=True)
@@ -203,7 +203,7 @@
             v_ref[rows, at] = (ref[rows, :].astype(f32) * factor * gain).astype(bf16)
         return 0
 
-    lax.fori_loop(0, ROWS // 128, normed, 0)
+    lax.fori_loop(0, ROWS // 64, normed, 0)
     gate_ref[...] = jnp.dot(
         v_ref[...], win_ref[:, 0:PIECE], preferred_element_type=f32
     ).astype(bf16)
@@ -245,7 +245,7 @@
     projected(hid_ref, turned_ref, wout_ref, outs)
 
 
-CHUNK = 128
+CHUNK = 256
 TOP = 16
 VMEM = pl.BlockSpec(memory_space=pltpu.VMEM)
 PARTS = tuple(jax.ShapeDtypeStruct((n * OWN, D), bf16) for n in (3, 1, 2, 2))

time: 188 us -> 188 us (level)
  no operation moved by 1% of the time
where the time goes in v3:
time: 188 us
  starting transfers between devices  88.4 us (47%)
  waiting for transfers between devices  60.1 us (32%)
  Pallas kernels  17.3 us (9%)
  blocking collectives  9.25 us (5%)
  other arithmetic  7.15 us (4%)
  local copies, waits for them, and re-layouts  5.04 us (3%)
    ppermute x9, starting transfers between devices, swapped(): return lax.ppermute(value, 'c', [(0, 1), (1, 0)])  45 us
    ppermute x12, waiting for transfers between devices, spread(): return lax.ppermute(value, (axis, 'c'), pairs)  40.5 us
    ppermute x16, starting transfers between devices, moved(): return lax.ppermute(value, axis, [(i, (i + by) % n) for i in range(n)])  23.7 us
    ppermute x12, starting transfers between devices, spread(): return lax.ppermute(value, (axis, 'c'), pairs)  15.7 us
    ppermute x16, waiting for transfers between devices, moved(): return lax.ppermute(value, axis, [(i, (i + by) % n) for i in range(n)])  14.1 us
    pallas_call x1, Pallas kernels, ffn(): pl.pallas_call(ffn_kernel, out_shape=PARTS, in_specs=[VMEM] * 8, out_spec...  9.57 us
    all_to_all x1, blocking collectives, shards(): return lax.all_to_all(to_columns, TP, 0, 0, tiled=True).reshape(ROWS, PIECE)  9.25 us
    pallas_call x1, Pallas kernels, mixer(): pl.pallas_call(mixer_kernel, out_shape=(*PARTS, PAIR, jax.ShapeDtypeStruc...  7.56 us
  transfers between devices with their start and end apart: 38, of which 16 were waited for; matrix products, arithmetic and copies ran while one was open for 5% of the time, Pallas kernels for 4%

profile of v3, /device:TPU:1, one launch (start us, length us, event | category | flops | bytes accessed | tf_op | source)
XLA Modules:
  0.0 187.6 jit_solution(7463467150249712177)
XLA Ops:
  0.9 2.5 %collective-permute-start.5 = (bf16[64,1472]{1,0:T(8,128)(2,1)S(1)}, bf16[64,1472]{1,0:T(8,128)(2,1)S(1)}, u32[]{:S(2)}, u32[]{:S(2)}) collective-permute-start(bf16[64,1472]{1,0:T(8,128)(2,1)S(1)} %pad_maximum_fusion.4.refs_0_), channel_id=1, source_target_pairs={{0,32},{32,64},{64,96},{96,128},{128,160},{160,192},{192,224},{224... | collective-permute-start | bytes 565256 | tf_op jit(solution)/shard_map/ppermute | solution.py:26
  3.5 4.0 %collective-permute-start.8 = (bf16[64,1472]{1,0:T(8,128)(2,1)S(1)}, bf16[64,1472]{1,0:T(8,128)(2,1)S(1)}, u32[]{:S(2)}, u32[]{:S(2)}) collective-permute-start(bf16[64,1472]{1,0:T(8,128)(2,1)S(1)} %pad_maximum_fusion.4.refs_0_), channel_id=1, source_target_pairs={{0,224},{32,0},{64,32},{96,64},{128,96},{160,128},{192,160},{224,1... | collective-permute-start | bytes 565256 | tf_op jit(solution)/shard_map/ppermute | solution.py:26
  9.5 4.0 %all-to-all-start = ((bf16[4,64,1408]{2,1,0:T(8,128)(2,1)}), bf16[4,64,1408]{2,1,0:T(8,128)(2,1)S(1)}, u32[]{:S(2)}, u32[]{:S(2)}) async-start(bf16[4,64,1408]{2,1,0:T(8,128)(2,1)} %broadcast_in_dim.56), calls=%async_computation | async-start | bytes 1441792 | tf_op jit(solution)/shard_map/all_to_all | solution.py:362
  16.5 2.7 %collective-permute-start.9 = (bf16[64,1472]{1,0:T(8,128)(2,1)S(1)}, bf16[64,1472]{1,0:T(8,128)(2,1)S(1)}, u32[]{:S(2)}, u32[]{:S(2)}) collective-permute-start(bf16[64,1472]{1,0:T(8,128)(2,1)S(1)} %collective-permute-done.8.refs_7_), channel_id=1, source_target_pairs={{0,224},{32,0},{64,32},{96,64},{128,96},{160,128},{192,160},{224,1... | collective-permute-start | bytes 565256 | tf_op jit(solution)/shard_map/ppermute | solution.py:26
  19.2 4.9 %collective-permute-done.6.refs_2_ = bf16[64,1472]{1,0:T(8,128)(2,1)S(1)} collective-permute-done((bf16[64,1472]{1,0:T(8,128)(2,1)S(1)}, bf16[64,1472]{1,0:T(8,128)(2,1)S(1)}, u32[]{:S(2)}, u32[]{:S(2)}) %collective-permute-start.6) | collective-permute-done | bytes 188448 | tf_op jit(solution)/shard_map/ppermute | solution.py:26
  24.1 2.7 %collective-permute-start.10 = (bf16[64,1472]{1,0:T(8,128)(2,1)S(1)}, bf16[64,1472]{1,0:T(8,128)(2,1)S(1)}, u32[]{:S(2)}, u32[]{:S(2)}) collective-permute-start(bf16[64,1472]{1,0:T(8,128)(2,1)S(1)} %collective-permute-done.9.refs_6_), channel_id=1, source_target_pairs={{0,224},{32,0},{64,32},{96,64},{128,96},{160,128},{192,160},{224,1... | collective-permute-start | bytes 565256 | tf_op jit(solution)/shard_map/ppermute | solution.py:26
  26.8 2.8 %collective-permute-start.1 = (bf16[2,528,256]{2,1,0:T(8,128)(2,1)S(1)}, bf16[2,528,256]{2,1,0:T(8,128)(2,1)S(1)}, u32[]{:S(2)}, u32[]{:S(2)}) collective-permute-start(bf16[2,528,256]{2,1,0:T(8,128)(2,1)S(1)} %pad_maximum_fusion.refs_0_), channel_id=1, source_target_pairs={{0,2},{2,4},{4,6},{6,0},{1,7},{3,1},{5,3},{7,5},{8,10},{10,12},{12... | collective-permute-start | bytes 1622024 | tf_op jit(solution)/shard_map/ppermute | solution.py:60
  31.5 2.4 %collective-permute-start.11 = (bf16[64,1472]{1,0:T(8,128)(2,1)}, bf16[64,1472]{1,0:T(8,128)(2,1)S(1)}, u32[]{:S(2)}, u32[]{:S(2)}) collective-permute-start(bf16[64,1472]{1,0:T(8,128)(2,1)} %broadcast_select_fusion.3), channel_id=1, source_target_pairs={{0,32},{32,64},{64,96},{96,128},{128,160},{160,192},{192,224},{224... | collective-permute-start | bytes 565256 | tf_op jit(solution)/shard_map/ppermute | solution.py:60
  33.9 2.9 %collective-permute-done.11.refs_4_ = bf16[64,1472]{1,0:T(8,128)(2,1)S(1)} collective-permute-done((bf16[64,1472]{1,0:T(8,128)(2,1)}, bf16[64,1472]{1,0:T(8,128)(2,1)S(1)}, u32[]{:S(2)}, u32[]{:S(2)}) %collective-permute-start.11) | collective-permute-done | bytes 188448 | tf_op jit(solution)/shard_map/ppermute | solution.py:60
  37.0 1.8 collective-permute-start.12
  40.3 8.0 %collective-permute-done.23 = bf16[4,64,1408]{2,1,0:T(8,128)(2,1)} collective-permute-done((bf16[4,64,1408]{2,1,0:T(8,128)(2,1)S(1)}, bf16[4,64,1408]{2,1,0:T(8,128)(2,1)}, u32[]{:S(2)}, u32[]{:S(2)}) %collective-permute-start.23) | collective-permute-done | bytes 720928 | tf_op jit(solution)/shard_map/ppermute | solution.py:26
  48.3 3.0 %collective-permute-start.31 = (bf16[8,64,704]{2,1,0:T(8,128)(2,1)S(1)}, bf16[8,64,704]{2,1,0:T(8,128)(2,1)S(1)}, u32[]{:S(2)}, u32[]{:S(2)}) collective-permute-start(bf16[8,64,704]{2,1,0:T(8,128)(2,1)S(1)} %get-tuple-element.32), channel_id=1, source_target_pairs={{0,24},{8,0},{16,8},{24,16},{1,25},{9,1},{17,9},{25,17},{2,26},{10... | collective-permute-start | bytes 2162696 | tf_op jit(solution)/shard_map/ppermute | solution.py:26
  55.5 3.5 %collective-permute-done.2.refs_2_ = bf16[528,256]{1,0:T(8,128)(2,1)S(1)} collective-permute-done((bf16[528,256]{1,0:T(8,128)(2,1)S(1)}, bf16[528,256]{1,0:T(8,128)(2,1)S(1)}, u32[]{:S(2)}, u32[]{:S(2)}) %collective-permute-start.2) | collective-permute-done | bytes 270368 | tf_op jit(solution)/shard_map/ppermute | solution.py:60
  58.9 17.0 %collective-permute-start.3 = (bf16[2,528,256]{2,1,0:T(8,128)(2,1)S(1)}, bf16[2,528,256]{2,1,0:T(8,128)(2,1)S(1)}, u32[]{:S(2)}, u32[]{:S(2)}) collective-permute-start(bf16[2,528,256]{2,1,0:T(8,128)(2,1)S(1)} %collective-permute-done.1.refs_1_), channel_id=1, source_target_pairs={{0,1},{1,0},{2,3},{3,2},{4,5},{5,4},{6,7},{7,6},{8,9},{9,8},{10,11... | collective-permute-start | bytes 1622024 | tf_op jit(solution)/shard_map/ppermute | solution.py:54
  76.3 2.7 %collective-permute-start.26 = (bf16[4,64,1408]{2,1,0:T(8,128)(2,1)S(1)}, bf16[4,64,1408]{2,1,0:T(8,128)(2,1)S(1)}, u32[]{:S(2)}, u32[]{:S(2)}) collective-permute-start(bf16[4,64,1408]{2,1,0:T(8,128)(2,1)S(1)} %collective-permute-done.24), channel_id=1, source_target_pairs={{0,224},{32,0},{64,32},{96,64},{128,96},{160,128},{192,160},{224,1... | collective-permute-start | bytes 2162696 | tf_op jit(solution)/shard_map/ppermute | solution.py:26
  79.0 1.6 collective-permute-start.32
  81.5 7.6 %mixer.1 = (bf16[192,2048]{1,0:T(8,128)(2,1)S(1)}, bf16[64,2048]{1,0:T(8,128)(2,1)S(1)}, bf16[128,2048]{1,0:T(8,128)(2,1)S(1)}, bf16[128,2048]{1,0:T(8,128)(2,1)...) custom-call(bf16[2,528,256]{2,1,0:T(8,128)(2,1)S(1)} %pad_maximum_fusion.refs_0_, ...), custom_call_target="tpu_custom_call" | custom-call | flops 1744830464 | bytes 8388608 | tf_op jit(solution)/shard_map/mixer/pallas_call | solution.py:256
  89.1 10.9 %collective-permute-start.15 = (bf16[192,2048]{1,0:T(8,128)(2,1)S(1)}, bf16[192,2048]{1,0:T(8,128)(2,1)S(1)}, u32[]{:S(2)}, u32[]{:S(2)}) collective-permute-start(bf16[192,2048]{1,0:T(8,128)(2,1)S(1)} %get-tuple-element.28), channel_id=1, source_target_pairs={{0,1},{1,0},{2,3},{3,2},{4,5},{5,4},{6,7},{7,6},{8,9},{9,8},{10,11... | collective-permute-start | bytes 2359304 | tf_op jit(solution)/shard_map/ppermute | solution.py:54
  101.2 2.2 %collective-permute-start.28 = (bf16[4,64,1408]{2,1,0:T(8,128)(2,1)S(1)}, bf16[4,64,1408]{2,1,0:T(8,128)(2,1)S(1)}, u32[]{:S(2)}, u32[]{:S(2)}) collective-permute-start(bf16[4,64,1408]{2,1,0:T(8,128)(2,1)S(1)} %collective-permute-done.26), channel_id=1, source_target_pairs={{0,224},{32,0},{64,32},{96,64},{128,96},{160,128},{192,160},{224,1... | collective-permute-start | bytes 2162696 | tf_op jit(solution)/shard_map/ppermute | solution.py:26
  105.2 4.0 %collective-permute-done.16 = bf16[64,2048]{1,0:T(8,128)(2,1)S(1)} collective-permute-done((bf16[64,2048]{1,0:T(8,128)(2,1)S(1)}, bf16[64,2048]{1,0:T(8,128)(2,1)S(1)}, u32[]{:S(2)}, u32[]{:S(2)}) %collective-permute-start.16) | collective-permute-done | bytes 262176 | tf_op jit(solution)/shard_map/ppermute | solution.py:60
  109.3 2.9 %collective-permute-start.17 = (bf16[128,2048]{1,0:T(8,128)(2,1)S(1)}, bf16[128,2048]{1,0:T(8,128)(2,1)S(1)}, u32[]{:S(2)}, u32[]{:S(2)}) collective-permute-start(bf16[128,2048]{1,0:T(8,128)(2,1)S(1)} %pad_maximum_fusion.1), channel_id=1, source_target_pairs={{0,2},{2,4},{4,6},{6,0},{1,7},{3,1},{5,3},{7,5},{8,10},{10,12},{12... | collective-permute-start | bytes 1572872 | tf_op jit(solution)/shard_map/ppermute | solution.py:60
  112.4 5.9 %collective-permute-done.17 = bf16[128,2048]{1,0:T(8,128)(2,1)S(1)} collective-permute-done((bf16[128,2048]{1,0:T(8,128)(2,1)S(1)}, bf16[128,2048]{1,0:T(8,128)(2,1)S(1)}, u32[]{:S(2)}, u32[]{:S(2)}) %collective-permute-start.17) | collective-permute-done | bytes 524320 | tf_op jit(solution)/shard_map/ppermute | solution.py:60
  118.5 4.4 %collective-permute-start.18 = (bf16[128,2048]{1,0:T(8,128)(2,1)S(1)}, bf16[128,2048]{1,0:T(8,128)(2,1)S(1)}, u32[]{:S(2)}, u32[]{:S(2)}) collective-permute-start(bf16[128,2048]{1,0:T(8,128)(2,1)S(1)} %pad_maximum_fusion.2), channel_id=1, source_target_pairs={{0,1},{1,0},{2,3},{3,2},{4,5},{5,4},{6,7},{7,6},{8,9},{9,8},{10,11... | collective-permute-start | bytes 1572872 | tf_op jit(solution)/shard_map/ppermute | solution.py:54
  125.8 8.0 %collective-permute-done.19.refs_1_ = bf16[2,64,2048]{2,1,0:T(8,128)(2,1)S(1)} collective-permute-done((bf16[2,64,2048]{2,1,0:T(8,128)(2,1)S(1)}, bf16[2,64,2048]{2,1,0:T(8,128)(2,1)S(1)}, u32[]{:S(2)}, u32[]{:S(2)}) %collective-permute-start.19) | collective-permute-done | bytes 524320 | tf_op jit(solution)/shard_map/ppermute | solution.py:60
  136.5 2.6 %collective-permute-done.20.refs_2_ = bf16[64,2048]{1,0:T(8,128)(2,1)S(1)} collective-permute-done((bf16[64,2048]{1,0:T(8,128)(2,1)S(1)}, bf16[64,2048]{1,0:T(8,128)(2,1)S(1)}, u32[]{:S(2)}, u32[]{:S(2)}) %collective-permute-start.20) | collective-permute-done | bytes 262176 | tf_op jit(solution)/shard_map/ppermute | solution.py:60
  139.1 4.8 %collective-permute-start.22 = (bf16[64,2048]{1,0:T(8,128)(2,1)S(1)}, bf16[64,2048]{1,0:T(8,128)(2,1)S(1)}, u32[]{:S(2)}, u32[]{:S(2)}) collective-permute-start(bf16[64,2048]{1,0:T(8,128)(2,1)S(1)} %collective-permute-done.20.refs_2_), channel_id=1, source_target_pairs={{0,1},{1,0},{2,3},{3,2},{4,5},{5,4},{6,7},{7,6},{8,9},{9,8},{10,11... | collective-permute-start | bytes 786440 | tf_op jit(solution)/shard_map/ppermute | solution.py:54
  145.1 9.6 %ffn.1 = (bf16[192,2048]{1,0:T(8,128)(2,1)S(1)}, bf16[64,2048]{1,0:T(8,128)(2,1)S(1)}, bf16[128,2048]{1,0:T(8,128)(2,1)S(1)}, bf16[128,2048]{1,0:T(8,128)(2,1)S(1)}) custom-call(bf16[2,64,2048]{2,1,0:T(8,128)(2,1)S(1)} %bitcast.61, bf16[2,64,2048]{2,1,0:T(8,128)(2,1)S(1)} %collective-permute-done.19.refs_1_, ...), custom_call_target="tpu_custom_call" | custom-call | flops 4429185024 | bytes 13631488 | tf_op jit(solution)/shard_map/ffn/pallas_call | solution.py:326
  155.1 1.9 %collective-permute-done.33 = bf16[192,2048]{1,0:T(8,128)(2,1)S(1)} collective-permute-done((bf16[192,2048]{1,0:T(8,128)(2,1)S(1)}, bf16[192,2048]{1,0:T(8,128)(2,1)S(1)}, u32[]{:S(2)}, u32[]{:S(2)}) %collective-permute-start.33) | collective-permute-done | bytes 786464 | tf_op jit(solution)/shard_map/ppermute | solution.py:54
  157.5 5.3 %collective-permute-done.34 = bf16[64,2048]{1,0:T(8,128)(2,1)S(1)} collective-permute-done((bf16[64,2048]{1,0:T(8,128)(2,1)S(1)}, bf16[64,2048]{1,0:T(8,128)(2,1)S(1)}, u32[]{:S(2)}, u32[]{:S(2)}) %collective-permute-start.34) | collective-permute-done | bytes 262176 | tf_op jit(solution)/shard_map/ppermute | solution.py:60
  164.0 7.4 %collective-permute-done.35 = bf16[128,2048]{1,0:T(8,128)(2,1)S(1)} collective-permute-done((bf16[128,2048]{1,0:T(8,128)(2,1)S(1)}, bf16[128,2048]{1,0:T(8,128)(2,1)S(1)}, u32[]{:S(2)}, u32[]{:S(2)}) %collective-permute-start.35) | collective-permute-done | bytes 524320 | tf_op jit(solution)/shard_map/ppermute | solution.py:60
  171.5 4.6 %collective-permute-start.36 = (bf16[64,2048]{1,0:T(8,128)(2,1)S(1)}, bf16[64,2048]{1,0:T(8,128)(2,1)S(1)}, u32[]{:S(2)}, u32[]{:S(2)}) collective-permute-start(bf16[64,2048]{1,0:T(8,128)(2,1)S(1)} %slice.86), channel_id=1, source_target_pairs={{0,1},{1,0},{2,3},{3,2},{4,5},{5,4},{6,7},{7,6},{8,9},{9,8},{10,11... | collective-permute-start | bytes 786440 | tf_op jit(solution)/shard_map/ppermute | solution.py:54
  177.7 9.2 %all_to_all.10 = bf16[8,64,256]{2,1,0:T(8,128)(2,1)S(1)} all-to-all(bf16[8,64,256]{2,1,0:T(8,128)(2,1)S(1)} %bitcast.65), channel_id=1, replica_groups=mesh['z'=8,'x'=4,'y'=4,'c'=2] {'y','c'}, dimensions={0} | all-to-all | bytes 524288 | tf_op jit(solution)/shard_map/all_to_all | solution.py:382
  (117 shorter events, 29.3 us)
Async XLA Ops:
  0.9 15.6 %collective-permute-start.5 = (bf16[64,1472]{1,0:T(8,128)(2,1)S(1)}, bf16[64,1472]{1,0:T(8,128)(2,1)S(1)}, u32[]{:S(2)}, u32[]{:S(2)}) collective-permute-start(bf16[64,1472]{1,0:T(8,128)(2,1)S(1)} %pad_maximum_fusion.4.refs_0_), channel_id=1, source_target_pairs={{0,32},{32,64},{64,96},{96,128},{128,160},{160,192},{192,224},{224... | collective-permute-start | bytes 565256 | tf_op jit(solution)/shard_map/ppermute | solution.py:26
  3.5 13.0 %collective-permute-start.8 = (bf16[64,1472]{1,0:T(8,128)(2,1)S(1)}, bf16[64,1472]{1,0:T(8,128)(2,1)S(1)}, u32[]{:S(2)}, u32[]{:S(2)}) collective-permute-start(bf16[64,1472]{1,0:T(8,128)(2,1)S(1)} %pad_maximum_fusion.4.refs_0_), channel_id=1, source_target_pairs={{0,224},{32,0},{64,32},{96,64},{128,96},{160,128},{192,160},{224,1... | collective-permute-start | bytes 565256 | tf_op jit(solution)/shard_map/ppermute | solution.py:26
  9.5 20.2 %all-to-all-start = ((bf16[4,64,1408]{2,1,0:T(8,128)(2,1)}), bf16[4,64,1408]{2,1,0:T(8,128)(2,1)S(1)}, u32[]{:S(2)}, u32[]{:S(2)}) async-start(bf16[4,64,1408]{2,1,0:T(8,128)(2,1)} %broadcast_in_dim.56), calls=%async_computation | async-start | bytes 1441792 | tf_op jit(solution)/shard_map/all_to_all | solution.py:362
  15.2 11.6 %collective-permute-start = (bf16[528,256]{1,0:T(8,128)(2,1)S(1)}, bf16[528,256]{1,0:T(8,128)(2,1)S(1)}, u32[]{:S(2)}, u32[]{:S(2)}) collective-permute-start(bf16[528,256]{1,0:T(8,128)(2,1)S(1)} %get-tuple-element.44), channel_id=1, source_target_pairs={{0,1},{1,0},{2,3},{3,2},{4,5},{5,4},{6,7},{7,6},{8,9},{9,8},{10,11... | collective-permute-start | bytes 811016 | tf_op jit(solution)/shard_map/ppermute | solution.py:54
  16.5 7.6 %collective-permute-start.6 = (bf16[64,1472]{1,0:T(8,128)(2,1)S(1)}, bf16[64,1472]{1,0:T(8,128)(2,1)S(1)}, u32[]{:S(2)}, u32[]{:S(2)}) collective-permute-start(bf16[64,1472]{1,0:T(8,128)(2,1)S(1)} %collective-permute-done.5.refs_1_), channel_id=1, source_target_pairs={{0,32},{32,64},{64,96},{96,128},{128,160},{160,192},{192,224},{224... | collective-permute-start | bytes 565256 | tf_op jit(solution)/shard_map/ppermute | solution.py:26
  16.5 7.6 %collective-permute-start.9 = (bf16[64,1472]{1,0:T(8,128)(2,1)S(1)}, bf16[64,1472]{1,0:T(8,128)(2,1)S(1)}, u32[]{:S(2)}, u32[]{:S(2)}) collective-permute-start(bf16[64,1472]{1,0:T(8,128)(2,1)S(1)} %collective-permute-done.8.refs_7_), channel_id=1, source_target_pairs={{0,224},{32,0},{64,32},{96,64},{128,96},{160,128},{192,160},{224,1... | collective-permute-start | bytes 565256 | tf_op jit(solution)/shard_map/ppermute | solution.py:26
  24.1 6.7 %collective-permute-start.7 = (bf16[64,1472]{1,0:T(8,128)(2,1)S(1)}, bf16[64,1472]{1,0:T(8,128)(2,1)S(1)}, u32[]{:S(2)}, u32[]{:S(2)}) collective-permute-start(bf16[64,1472]{1,0:T(8,128)(2,1)S(1)} %collective-permute-done.6.refs_2_), channel_id=1, source_target_pairs={{0,32},{32,64},{64,96},{96,128},{128,160},{160,192},{192,224},{224... | collective-permute-start | bytes 565256 | tf_op jit(solution)/shard_map/ppermute | solution.py:26
  24.1 6.7 %collective-permute-start.10 = (bf16[64,1472]{1,0:T(8,128)(2,1)S(1)}, bf16[64,1472]{1,0:T(8,128)(2,1)S(1)}, u32[]{:S(2)}, u32[]{:S(2)}) collective-permute-start(bf16[64,1472]{1,0:T(8,128)(2,1)S(1)} %collective-permute-done.9.refs_6_), channel_id=1, source_target_pairs={{0,224},{32,0},{64,32},{96,64},{128,96},{160,128},{192,160},{224,1... | collective-permute-start | bytes 565256 | tf_op jit(solution)/shard_map/ppermute | solution.py:26
  26.8 13.3 %collective-permute-start.1 = (bf16[2,528,256]{2,1,0:T(8,128)(2,1)S(1)}, bf16[2,528,256]{2,1,0:T(8,128)(2,1)S(1)}, u32[]{:S(2)}, u32[]{:S(2)}) collective-permute-start(bf16[2,528,256]{2,1,0:T(8,128)(2,1)S(1)} %pad_maximum_fusion.refs_0_), channel_id=1, source_target_pairs={{0,2},{2,4},{4,6},{6,0},{1,7},{3,1},{5,3},{7,5},{8,10},{10,12},{12... | collective-permute-start | bytes 1622024 | tf_op jit(solution)/shard_map/ppermute | solution.py:60
  29.6 18.7 %collective-permute-start.23 = (bf16[4,64,1408]{2,1,0:T(8,128)(2,1)S(1)}, bf16[4,64,1408]{2,1,0:T(8,128)(2,1)}, u32[]{:S(2)}, u32[]{:S(2)}) collective-permute-start(bf16[4,64,1408]{2,1,0:T(8,128)(2,1)S(1)} %all-to-all-done), channel_id=1, source_target_pairs={{0,32},{32,64},{64,96},{96,128},{128,160},{160,192},{192,224},{224... | collective-permute-start | bytes 2162696 | tf_op jit(solution)/shard_map/ppermute | solution.py:26
  33.9 42.1 %collective-permute-start.24 = (bf16[4,64,1408]{2,1,0:T(8,128)(2,1)S(1)}, bf16[4,64,1408]{2,1,0:T(8,128)(2,1)S(1)}, u32[]{:S(2)}, u32[]{:S(2)}) collective-permute-start(bf16[4,64,1408]{2,1,0:T(8,128)(2,1)S(1)} %all-to-all-done), channel_id=1, source_target_pairs={{0,224},{32,0},{64,32},{96,64},{128,96},{160,128},{192,160},{224,1... | collective-permute-start | bytes 2162696 | tf_op jit(solution)/shard_map/ppermute | solution.py:26
  37.0 16.3 %collective-permute-start.12 = (bf16[8,64,768]{2,1,0:T(8,128)(2,1)S(1)}, bf16[8,64,768]{2,1,0:T(8,128)(2,1)S(1)}, u32[]{:S(2)}, u32[]{:S(2)}) collective-permute-start(bf16[8,64,768]{2,1,0:T(8,128)(2,1)S(1)} %get-tuple-element.23.refs_5_), channel_id=1, source_target_pairs={{0,8},{8,16},{16,24},{24,0},{1,9},{9,17},{17,25},{25,1},{2,10},{10... | collective-permute-start | bytes 2359304 | tf_op jit(solution)/shard_map/ppermute | solution.py:26
  38.8 15.8 %collective-permute-start.13 = (bf16[8,64,768]{2,1,0:T(8,128)(2,1)S(1)}, bf16[8,64,768]{2,1,0:T(8,128)(2,1)S(1)}, u32[]{:S(2)}, u32[]{:S(2)}) collective-permute-start(bf16[8,64,768]{2,1,0:T(8,128)(2,1)S(1)} %get-tuple-element.23.refs_5_), channel_id=1, source_target_pairs={{0,24},{8,0},{16,8},{24,16},{1,25},{9,1},{17,9},{25,17},{2,26},{10... | collective-permute-start | bytes 2359304 | tf_op jit(solution)/shard_map/ppermute | solution.py:26
  40.1 36.1 %collective-permute-start.30 = (bf16[8,64,704]{2,1,0:T(8,128)(2,1)S(1)}, bf16[8,64,704]{2,1,0:T(8,128)(2,1)S(1)}, u32[]{:S(2)}, u32[]{:S(2)}) collective-permute-start(bf16[8,64,704]{2,1,0:T(8,128)(2,1)S(1)} %get-tuple-element.32), channel_id=1, source_target_pairs={{0,8},{8,16},{16,24},{24,0},{1,9},{9,17},{17,25},{25,1},{2,10},{10... | collective-permute-start | bytes 2162696 | tf_op jit(solution)/shard_map/ppermute | solution.py:26
  48.3 28.0 %collective-permute-start.31 = (bf16[8,64,704]{2,1,0:T(8,128)(2,1)S(1)}, bf16[8,64,704]{2,1,0:T(8,128)(2,1)S(1)}, u32[]{:S(2)}, u32[]{:S(2)}) collective-permute-start(bf16[8,64,704]{2,1,0:T(8,128)(2,1)S(1)} %get-tuple-element.32), channel_id=1, source_target_pairs={{0,24},{8,0},{16,8},{24,16},{1,25},{9,1},{17,9},{25,17},{2,26},{10... | collective-permute-start | bytes 2162696 | tf_op jit(solution)/shard_map/ppermute | solution.py:26
  53.3 5.7 %collective-permute-start.2 = (bf16[528,256]{1,0:T(8,128)(2,1)S(1)}, bf16[528,256]{1,0:T(8,128)(2,1)S(1)}, u32[]{:S(2)}, u32[]{:S(2)}) collective-permute-start(bf16[528,256]{1,0:T(8,128)(2,1)S(1)} %slice_bitcast_fusion), channel_id=1, source_target_pairs={{0,2},{2,4},{4,6},{6,0},{1,7},{3,1},{5,3},{7,5},{8,10},{10,12},{12... | collective-permute-start | bytes 811016 | tf_op jit(solution)/shard_map/ppermute | solution.py:60
  54.7 26.8 %collective-permute-start.14 = (bf16[8,64,768]{2,1,0:T(8,128)(2,1)S(1)}, bf16[8,64,768]{2,1,0:T(8,128)(2,1)S(1)}, u32[]{:S(2)}, u32[]{:S(2)}) collective-permute-start(bf16[8,64,768]{2,1,0:T(8,128)(2,1)S(1)} %broadcast_select_fusion.1), channel_id=1, source_target_pairs={{0,8},{8,16},{16,24},{24,0},{1,25},{9,1},{17,9},{25,17},{2,10},{10... | collective-permute-start | bytes 2359304 | tf_op jit(solution)/shard_map/ppermute | solution.py:60
  58.9 20.1 %collective-permute-start.3 = (bf16[2,528,256]{2,1,0:T(8,128)(2,1)S(1)}, bf16[2,528,256]{2,1,0:T(8,128)(2,1)S(1)}, u32[]{:S(2)}, u32[]{:S(2)}) collective-permute-start(bf16[2,528,256]{2,1,0:T(8,128)(2,1)S(1)} %collective-permute-done.1.refs_1_), channel_id=1, source_target_pairs={{0,1},{1,0},{2,3},{3,2},{4,5},{5,4},{6,7},{7,6},{8,9},{9,8},{10,11... | collective-permute-start | bytes 1622024 | tf_op jit(solution)/shard_map/ppermute | solution.py:54
  76.2 24.4 %collective-permute-start.25 = (bf16[4,64,1408]{2,1,0:T(8,128)(2,1)}, bf16[4,64,1408]{2,1,0:T(8,128)(2,1)S(1)}, u32[]{:S(2)}, u32[]{:S(2)}) collective-permute-start(bf16[4,64,1408]{2,1,0:T(8,128)(2,1)} %collective-permute-done.23), channel_id=1, source_target_pairs={{0,32},{32,64},{64,96},{96,128},{128,160},{160,192},{192,224},{224... | collective-permute-start | bytes 2162696 | tf_op jit(solution)/shard_map/ppermute | solution.py:26
  76.3 24.9 %collective-permute-start.26 = (bf16[4,64,1408]{2,1,0:T(8,128)(2,1)S(1)}, bf16[4,64,1408]{2,1,0:T(8,128)(2,1)S(1)}, u32[]{:S(2)}, u32[]{:S(2)}) collective-permute-start(bf16[4,64,1408]{2,1,0:T(8,128)(2,1)S(1)} %collective-permute-done.24), channel_id=1, source_target_pairs={{0,224},{32,0},{64,32},{96,64},{128,96},{160,128},{192,160},{224,1... | collective-permute-start | bytes 2162696 | tf_op jit(solution)/shard_map/ppermute | solution.py:26
  79.0 43.9 %collective-permute-start.32 = (bf16[8,64,704]{2,1,0:T(8,128)(2,1)S(1)}, bf16[8,64,704]{2,1,0:T(8,128)(2,1)S(1)}, u32[]{:S(2)}, u32[]{:S(2)}) collective-permute-start(bf16[8,64,704]{2,1,0:T(8,128)(2,1)S(1)} %broadcast_select_fusion), channel_id=1, source_target_pairs={{0,8},{8,16},{16,24},{24,0},{1,25},{9,1},{17,9},{25,17},{2,10},{10... | collective-permute-start | bytes 2162696 | tf_op jit(solution)/shard_map/ppermute | solution.py:60
  89.1 14.3 %collective-permute-start.15 = (bf16[192,2048]{1,0:T(8,128)(2,1)S(1)}, bf16[192,2048]{1,0:T(8,128)(2,1)S(1)}, u32[]{:S(2)}, u32[]{:S(2)}) collective-permute-start(bf16[192,2048]{1,0:T(8,128)(2,1)S(1)} %get-tuple-element.28), channel_id=1, source_target_pairs={{0,1},{1,0},{2,3},{3,2},{4,5},{5,4},{6,7},{7,6},{8,9},{9,8},{10,11... | collective-permute-start | bytes 2359304 | tf_op jit(solution)/shard_map/ppermute | solution.py:54
  100.6 24.9 %collective-permute-start.27 = (bf16[4,64,1408]{2,1,0:T(8,128)(2,1)S(1)}, bf16[4,64,1408]{2,1,0:T(8,128)(2,1)S(1)}, u32[]{:S(2)}, u32[]{:S(2)}) collective-permute-start(bf16[4,64,1408]{2,1,0:T(8,128)(2,1)S(1)} %collective-permute-done.25), channel_id=1, source_target_pairs={{0,32},{32,64},{64,96},{96,128},{128,160},{160,192},{192,224},{224... | collective-permute-start | bytes 2162696 | tf_op jit(solution)/shard_map/ppermute | solution.py:26
  101.2 24.3 %collective-permute-start.28 = (bf16[4,64,1408]{2,1,0:T(8,128)(2,1)S(1)}, bf16[4,64,1408]{2,1,0:T(8,128)(2,1)S(1)}, u32[]{:S(2)}, u32[]{:S(2)}) collective-permute-start(bf16[4,64,1408]{2,1,0:T(8,128)(2,1)S(1)} %collective-permute-done.26), channel_id=1, source_target_pairs={{0,224},{32,0},{64,32},{96,64},{128,96},{160,128},{192,160},{224,1... | collective-permute-start | bytes 2162696 | tf_op jit(solution)/shard_map/ppermute | solution.py:26
  109.3 9.0 %collective-permute-start.17 = (bf16[128,2048]{1,0:T(8,128)(2,1)S(1)}, bf16[128,2048]{1,0:T(8,128)(2,1)S(1)}, u32[]{:S(2)}, u32[]{:S(2)}) collective-permute-start(bf16[128,2048]{1,0:T(8,128)(2,1)S(1)} %pad_maximum_fusion.1), channel_id=1, source_target_pairs={{0,2},{2,4},{4,6},{6,0},{1,7},{3,1},{5,3},{7,5},{8,10},{10,12},{12... | collective-permute-start | bytes 1572872 | tf_op jit(solution)/shard_map/ppermute | solution.py:60
  118.5 5.9 %collective-permute-start.18 = (bf16[128,2048]{1,0:T(8,128)(2,1)S(1)}, bf16[128,2048]{1,0:T(8,128)(2,1)S(1)}, u32[]{:S(2)}, u32[]{:S(2)}) collective-permute-start(bf16[128,2048]{1,0:T(8,128)(2,1)S(1)} %pad_maximum_fusion.2), channel_id=1, source_target_pairs={{0,1},{1,0},{2,3},{3,2},{4,5},{5,4},{6,7},{7,6},{8,9},{9,8},{10,11... | collective-permute-start | bytes 1572872 | tf_op jit(solution)/shard_map/ppermute | solution.py:54
  125.4 8.4 %collective-permute-start.19 = (bf16[2,64,2048]{2,1,0:T(8,128)(2,1)S(1)}, bf16[2,64,2048]{2,1,0:T(8,128)(2,1)S(1)}, u32[]{:S(2)}, u32[]{:S(2)}) collective-permute-start(bf16[2,64,2048]{2,1,0:T(8,128)(2,1)S(1)} %bitcast.60), channel_id=1, source_target_pairs={{0,2},{2,4},{4,6},{6,0},{1,7},{3,1},{5,3},{7,5},{8,10},{10,12},{12... | collective-permute-start | bytes 1572872 | tf_op jit(solution)/shard_map/ppermute | solution.py:60
  125.6 18.3 %collective-permute-start.29 = (bf16[4,64,1408]{2,1,0:T(8,128)(2,1)S(1)}, bf16[4,64,1408]{2,1,0:T(8,128)(2,1)S(1)}, u32[]{:S(2)}, u32[]{:S(2)}) collective-permute-start(bf16[4,64,1408]{2,1,0:T(8,128)(2,1)S(1)} %broadcast_select_fusion.2), channel_id=1, source_target_pairs={{0,32},{32,64},{64,96},{96,128},{128,160},{160,192},{192,224},{224... | collective-permute-start | bytes 2162696 | tf_op jit(solution)/shard_map/ppermute | solution.py:60
  135.2 8.9 %collective-permute-start.21 = (bf16[2,64,2048]{2,1,0:T(8,128)(2,1)S(1)}, bf16[2,64,2048]{2,1,0:T(8,128)(2,1)S(1)}, u32[]{:S(2)}, u32[]{:S(2)}) collective-permute-start(bf16[2,64,2048]{2,1,0:T(8,128)(2,1)S(1)} %collective-permute-done.19.refs_1_), channel_id=1, source_target_pairs={{0,1},{1,0},{2,3},{3,2},{4,5},{5,4},{6,7},{7,6},{8,9},{9,8},{10,11... | collective-permute-start | bytes 1572872 | tf_op jit(solution)/shard_map/ppermute | solution.py:54
  139.1 6.0 %collective-permute-start.22 = (bf16[64,2048]{1,0:T(8,128)(2,1)S(1)}, bf16[64,2048]{1,0:T(8,128)(2,1)S(1)}, u32[]{:S(2)}, u32[]{:S(2)}) collective-permute-start(bf16[64,2048]{1,0:T(8,128)(2,1)S(1)} %collective-permute-done.20.refs_2_), channel_id=1, source_target_pairs={{0,1},{1,0},{2,3},{3,2},{4,5},{5,4},{6,7},{7,6},{8,9},{9,8},{10,11... | collective-permute-start | bytes 786440 | tf_op jit(solution)/shard_map/ppermute | solution.py:54
  163.0 8.4 %collective-permute-start.35 = (bf16[128,2048]{1,0:T(8,128)(2,1)S(1)}, bf16[128,2048]{1,0:T(8,128)(2,1)S(1)}, u32[]{:S(2)}, u32[]{:S(2)}) collective-permute-start(bf16[128,2048]{1,0:T(8,128)(2,1)S(1)} %pad_maximum_fusion.3), channel_id=1, source_target_pairs={{0,2},{2,4},{4,6},{6,0},{1,7},{3,1},{5,3},{7,5},{8,10},{10,12},{12... | collective-permute-start | bytes 1572872 | tf_op jit(solution)/shard_map/ppermute | solution.py:60
  171.5 5.8 %collective-permute-start.36 = (bf16[64,2048]{1,0:T(8,128)(2,1)S(1)}, bf16[64,2048]{1,0:T(8,128)(2,1)S(1)}, u32[]{:S(2)}, u32[]{:S(2)}) collective-permute-start(bf16[64,2048]{1,0:T(8,128)(2,1)S(1)} %slice.86), channel_id=1, source_target_pairs={{0,1},{1,0},{2,3},{3,2},{4,5},{5,4},{6,7},{7,6},{8,9},{9,8},{10,11... | collective-permute-start | bytes 786440 | tf_op jit(solution)/shard_map/ppermute | solution.py:54
  (12 other events, 199.7 us)
